TPU v7x, 256 devices: a 2x2x32 block of a 4x16x32 slice. The times are simulated.
256 devices in a mesh: grp: 4 (over y, x), ep: 32 (over z), tp: 2 (over core).
Axes of the slice: x: 2, y: 2, z: 32, core: 2. Of those that a mesh axis runs over, the one named last changes fastest.
The devices are a block of a 4x16x32 slice.
Arguments:
- tokens: bfloat16 [4096, 2048], P(('grp', 'ep'), 'tp'), parts along dimension 0, may hold values from -6 to 6
- routes: int32 [4096, 4], P(('grp', 'ep')), parts along dimension 0, may hold values from 0 to 31, all different within a row; in each aligned block of 32 rows (0 to 31, 32 to 63, ...) at most 6 rows name the same one
- gate_logits: float32 [4096, 4], P(('grp', 'ep')), parts along dimension 0, may hold values from -6 to 6
- norm_gain: float32 [2048], P('tp'), may hold values from 0.1 to 1.9
- norm_shift: float32 [2048], P('tp'), may hold values from -3 to 3
- gate_weight: bfloat16 [32, 2048, 1024], P('ep', None, 'tp'), may hold values from -0.5 to 0.5
- up_weight: bfloat16 [32, 2048, 1024], P('ep', None, 'tp'), may hold values from -0.5 to 0.5
- down_weight: bfloat16 [32, 1024, 2048], P('ep', 'tp'), may hold values from -0.0234375 to 0.0234375
Outputs:
- mixed: bfloat16 [4096, 2048], P(('grp', 'ep'), 'tp'), parts along dimension 0
There are 4 independent parts, one for each index of `grp`. A program takes and returns all parts, laid end to end along the dimension named above; an argument that names none is the same for every part. Nothing has to cross between parts.
Inputs may be any that keep to these rules, and one draw needn't show every extreme that they name: `routes`: each row names 4 different experts. Within the 32 rows of one index of ep no expert is named more than 6 times, a bound that some blocks reach.
All inputs are finite; a program needn't handle non-finite values.
Results may differ from a plain program's by a relative error of at most 0.012.
Values may be sent and summed in bfloat16 or wider, within the bound.
No kernel may reach another device: no remote copies, remote signals or barrier semaphores. Data moves between devices by JAX's collectives and lax.ppermute only.
A program may use at most 64 MiB of HBM per device.

v0:
```python
import jax
import jax.numpy as jnp
from jax import lax
from jax.sharding import PartitionSpec as P

norm_eps = 1e-05
clamp_limit = 7.0
sigmoid_slope = 1.702


def in_order(pieces, dim):
    pieces = jnp.moveaxis(pieces, 0, dim)
    shape = pieces.shape
    return pieces.reshape(*shape[:dim], shape[dim] * shape[dim + 1], *shape[dim + 2 :])


def copy_for_each(x, axis):
    length = lax.axis_size(axis)
    return lax.all_to_all(jnp.broadcast_to(x[None], (length, *x.shape)), axis, 0, 0, tiled=True)


def gathered_copies(x, axis, dim):
    return in_order(copy_for_each(x, axis), dim)


def split_up(x, dim, length):
    before, after = (x.shape[:dim], x.shape[dim + 1 :])
    return jnp.moveaxis(x.reshape(*before, length, -1, *after), dim, 0)


def summed_on_arrival(x, axis, dim):
    length = lax.axis_size(axis)
    pieces = lax.all_to_all(split_up(x, dim, length), axis, 0, 0, tiled=True)
    return jnp.sum(pieces.astype(jnp.float32), axis=0)


def expert_apply(received, gate_weight, up_weight, down_weight):
    whole = gathered_copies(received, "tp", 2)
    sources, slots_here, width = whole.shape
    row_block = whole.reshape(sources * slots_here, width)
    gate_pre = jnp.dot(row_block, gate_weight[0], preferred_element_type=jnp.float32)
    up_pre = jnp.dot(row_block, up_weight[0], preferred_element_type=jnp.float32)
    gate_cut = jnp.minimum(gate_pre, clamp_limit)
    up_cut = jnp.clip(up_pre, -clamp_limit, clamp_limit)
    hidden = ((up_cut + 1.0) * gate_cut * jax.nn.sigmoid(sigmoid_slope * gate_cut)).astype(
        jnp.bfloat16
    )
    partial_out = jnp.dot(hidden, down_weight[0], preferred_element_type=jnp.float32).astype(
        jnp.bfloat16
    )
    summed = summed_on_arrival(partial_out.reshape(sources, slots_here, width), "tp", 2)
    return summed.astype(jnp.bfloat16)


def slot_ranks(flat_experts, expert_count):
    onehot = (flat_experts[:, None] == jnp.arange(expert_count, dtype=jnp.int32)[None, :]).astype(
        jnp.int32
    )
    earlier = jnp.cumsum(onehot, axis=0) - onehot
    return jnp.sum(earlier * onehot, axis=1)


def body(tokens, routes, gate_logits, norm_gain, norm_shift, gate_weight, up_weight, down_weight):
    ep_count = lax.axis_size("ep")
    tok_rows, top_count = routes.shape
    half_width = tokens.shape[1]
    full_width = half_width * lax.axis_size("tp")
    capacity = tok_rows * top_count // ep_count + 2
    floats = tokens.astype(jnp.float32)
    entire = gathered_copies(tokens, "tp", 1).astype(jnp.float32)
    row_sums = jnp.sum(entire, axis=1)
    row_squares = jnp.sum(entire * entire, axis=1)
    average = row_sums / full_width
    variance = row_squares / full_width - average * average
    normed = (
        (floats - average[:, None]) * lax.rsqrt(variance[:, None] + norm_eps) * norm_gain
        + norm_shift
    ).astype(jnp.bfloat16)
    send_width = normed.shape[1]
    exp_logits = jnp.exp(gate_logits)
    weights = exp_logits / jnp.sum(exp_logits, axis=1, keepdims=True)
    flat_experts = routes.reshape(-1)
    slot_index = flat_experts * capacity + slot_ranks(flat_experts, ep_count)
    token_index = jnp.arange(tok_rows * top_count, dtype=jnp.int32) // top_count
    outgoing = (
        jnp.zeros((ep_count * capacity, send_width), jnp.bfloat16)
        .at[slot_index]
        .set(normed[token_index])
    )
    answered = expert_apply(
        lax.all_to_all(
            outgoing.reshape(ep_count, capacity, send_width),
            "ep",
            split_axis=0,
            concat_axis=0,
            tiled=True,
        ),
        gate_weight,
        up_weight,
        down_weight,
    )
    returned = lax.all_to_all(answered, "ep", split_axis=0, concat_axis=0, tiled=True)
    picked = returned.reshape(ep_count * capacity, half_width)[slot_index].astype(jnp.float32)
    mixed = jnp.sum(picked.reshape(tok_rows, top_count, half_width) * weights[:, :, None], axis=1)
    return mixed.astype(jnp.bfloat16)


def solution(mesh):
    placed = (
        P(("grp", "ep"), "tp"),
        P(("grp", "ep"), None),
        P(("grp", "ep"), None),
        P("tp"),
        P("tp"),
        P("ep", None, "tp"),
        P("ep", None, "tp"),
        P("ep", "tp", None),
    )
    return jax.shard_map(
        body, mesh=mesh, in_specs=placed, out_specs=P(("grp", "ep"), "tp"), check_vma=False
    )
```

profile of v0, /device:TPU:166, one launch (start us, length us, event | category | flops | bytes accessed | tf_op | source)
XLA Modules:
  0.0 196.6 jit_solution(15458047361020289934)
XLA Ops:
  0.0 1.6 broadcast_in_dim.7
  1.6 3.4 %all-to-all-start = ((bf16[2,32,1024]{2,1,0:T(8,128)(2,1)}), bf16[2,32,1024]{2,1,0:T(8,128)(2,1)S(1)}, u32[]{:S(2)}, u32[]{:S(2)}) async-start(bf16[2,32,1024]{2,1,0:T(8,128)(2,1)} %broadcast_in_dim.7), calls=%async_computation | async-start | bytes 262144 | tf_op jit(solution)/shard_map/all_to_all | solution.py:19
  5.1 0.8 copy.41
  5.8 0.7 broadcast_multiply_fusion
  6.7 0.2 reduce_window_sum.11
  6.9 0.2 select_reduce_fusion
  7.5 0.9 add_convert_fusion
  8.4 2.1 %scatter_custom_fusion = bf16[192,1024]{1,0:T(8,128)(2,1)S(1)} fusion(s32[128]{0:T(128)S(1)} %fusion.40, bf16[32,1024]{1,0:T(8,128)(2,1)S(1)} %add_convert_fusion, s32[1024]{0:T(1024)S(1)} %pad_clamp_fusion.1, bf16[]{:T(256)} %constant.18.clone.1), kind=kCustom, calls=%fused_computation.25 | custom fusion | bytes 393218 | tf_op jit(solution)/shard_map/scatter | solution.py:88
  10.7 95.5 %all_to_all.25 = bf16[32,6,1024]{2,1,0:T(8,128)(2,1)S(1)} all-to-all(bf16[32,6,1024]{2,1,0:T(8,128)(2,1)S(1)} %reshape.104), channel_id=1, replica_groups=mesh['grp'=4,'ep'=32,'tp'=2] {'ep'}, dimensions={0} | all-to-all | bytes 786432 | tf_op jit(solution)/shard_map/all_to_all | solution.py:91
  106.2 0.2 copy.42
  106.5 4.5 %all_to_all.26 = bf16[2,32,6,1024]{3,1,2,0:T(8,128)(2,1)S(1)} all-to-all(bf16[2,32,6,1024]{3,1,2,0:T(8,128)(2,1)S(1)} %broadcast_in_dim.8), channel_id=1, replica_groups=mesh['grp'=4,'ep'=32,'tp'=2] {'tp'}, dimensions={0} | all-to-all | bytes 1572864 | tf_op jit(solution)/shard_map/all_to_all | solution.py:19
  111.0 0.8 copy.43
  111.8 0.2 copy.47
  112.0 0.6 fusion.17
  112.6 3.6 %convolution_convert_fusion = bf16[192,2048]{1,0:T(8,128)(2,1)} fusion(bf16[1,512,2048]{2,1,0:T(8,128)(2,1)S(1)} %copy-done, f32[192,512]{1,0:T(8,128)S(1)} %fusion.17, bf16[192,2048]{1,0:T(8,128)(2,1)S(1)} %bitcast.44, bf16[1,2048,512]{2,1,0:T(8,128)(2,1)} %param.14), kind=kOutput, calls=%fused_computation.3 | convolution fusion | flops 806584320 | bytes 6160384 | tf_op jit(solution)/shard_map/dot_general | solution.py:48
  116.3 2.6 %reshape_reshape.7 = bf16[32,6,2,1024]{3,2,1,0:T(2,128)(2,1)S(1)} reshape(bf16[192,2048]{1,0:T(8,128)(2,1)} %convolution_convert_fusion) | data formatting | bytes 1572864 | tf_op jit(solution)/shard_map/reshape;reshape | solution.py:28
  118.8 0.2 copy.49
  119.1 4.4 %all_to_all.27 = bf16[2,32,6,1024]{3,1,2,0:T(8,128)(2,1)S(1)} all-to-all(bf16[2,32,6,1024]{3,1,2,0:T(8,128)(2,1)S(1)} %bitcast.42), channel_id=1, replica_groups=mesh['grp'=4,'ep'=32,'tp'=2] {'tp'}, dimensions={0} | all-to-all | bytes 1572864 | tf_op jit(solution)/shard_map/all_to_all | solution.py:33
  123.6 1.0 copy.45
  124.7 5.6 %all-to-all-start.4 = ((bf16[32,6,1024]{2,1,0:T(8,128)(2,1)}), bf16[32,6,1024]{2,1,0:T(8,128)(2,1)S(1)}, u32[]{:S(2)}, u32[]{:S(2)}) async-start(bf16[32,6,1024]{2,1,0:T(8,128)(2,1)} %copy.45), calls=%async_computation.4 | async-start | bytes 1048576 | tf_op jit(solution)/shard_map/all_to_all | solution.py:102
  130.4 63.9 %all-to-all-done.4 = bf16[32,6,1024]{2,1,0:T(8,128)(2,1)S(1)} async-done(((bf16[32,6,1024]{2,1,0:T(8,128)(2,1)}), bf16[32,6,1024]{2,1,0:T(8,128)(2,1)S(1)}, u32[]{:S(2)}, u32[]{:S(2)}) %all-to-all-start.4) | async-done | bytes 393248 | tf_op jit(solution)/shard_map/all_to_all | solution.py:102
  194.5 0.9 gather_fusion
  195.4 0.2 reshape.106
  195.5 1.0 multiply_reduce_fusion
  (24 shorter events, 1.2 us)
Async XLA Ops:
  0.0 112.6 %copy-start = (bf16[1,512,2048]{2,1,0:T(8,128)(2,1)S(1)}, bf16[1,512,2048]{2,1,0:T(8,128)(2,1)}, u32[]{:S(2)}) copy-start(bf16[1,512,2048]{2,1,0:T(8,128)(2,1)} %param.15) | copy-start | bytes 6291460
  1.6 5.6 %all-to-all-start = ((bf16[2,32,1024]{2,1,0:T(8,128)(2,1)}), bf16[2,32,1024]{2,1,0:T(8,128)(2,1)S(1)}, u32[]{:S(2)}, u32[]{:S(2)}) async-start(bf16[2,32,1024]{2,1,0:T(8,128)(2,1)} %broadcast_in_dim.7), calls=%async_computation | async-start | bytes 262144 | tf_op jit(solution)/shard_map/all_to_all | solution.py:19
  106.5 5.5 %copy-start.1 = (bf16[1,2048,512]{2,1,0:T(8,128)(2,1)S(1)}, bf16[1,2048,512]{2,1,0:T(8,128)(2,1)}, u32[]{:S(2)}) copy-start(bf16[1,2048,512]{2,1,0:T(8,128)(2,1)} %param.13) | copy-start | bytes 6291460
  119.1 11.2 %copy-start.2 = (f32[32,4]{0,1:T(4,128)S(1)}, f32[32,4]{0,1:T(4,128)}, u32[]{:S(2)}) copy-start(f32[32,4]{0,1:T(4,128)} %param.10) | copy-start | bytes 1540
  124.7 69.7 %all-to-all-start.4 = ((bf16[32,6,1024]{2,1,0:T(8,128)(2,1)}), bf16[32,6,1024]{2,1,0:T(8,128)(2,1)S(1)}, u32[]{:S(2)}, u32[]{:S(2)}) async-start(bf16[32,6,1024]{2,1,0:T(8,128)(2,1)} %copy.45), calls=%async_computation.4 | async-start | bytes 1048576 | tf_op jit(solution)/shard_map/all_to_all | solution.py:102
where the time goes:
time: 199 us; the launch traced here: 197 us
  blocking collectives  104 us (52%)
  waiting for transfers between devices  63.9 us (32%)
  local copies, waits for them, and re-layouts  11.4 us (6%)
  starting transfers between devices  9.03 us (5%)
  matrix products  4.19 us (2%)
  other arithmetic  3.47 us (2%)
    all_to_all x1, blocking collectives, body(): lax.all_to_all(outgoing.reshape(ep_count, capacity, send_width), 'ep', sp...  95.5 us
    all_to_all x1, waiting for transfers between devices, body(): lax.all_to_all(answered, 'ep', split_axis=0, concat_axis=0, tiled=True)  63.9 us
    all_to_all x1, starting transfers between devices, body(): lax.all_to_all(answered, 'ep', split_axis=0, concat_axis=0, tiled=True)  5.62 us
    all_to_all x1, blocking collectives, copy_for_each(): lax.all_to_all(jnp.broadcast_to(x[None], (length, *x.shape)), axis, 0, 0,...  4.51 us
    all_to_all x1, blocking collectives, summed_on_arrival(): pieces = lax.all_to_all(split_up(x, dim, length), axis, 0, 0, tiled=True)  4.38 us
  transfers between devices with their start and end apart: 2, of which 1 were waited for; matrix products, arithmetic and copies ran while one was open for 1% of the time, Pallas kernels for 0%

commit v1 on v0

v1 whole, which is shorter than its diff:
```python
import jax
import jax.numpy as jnp
from jax import lax
from jax.sharding import PartitionSpec as P

norm_eps = 1e-05
clamp_limit = 7.0
sigmoid_slope = 1.702
lanes = 128


def swap_tp(x):
    return lax.ppermute(x, "tp", [(0, 1), (1, 0)])


def exchange(x):
    return lax.all_to_all(x, "ep", split_axis=0, concat_axis=0, tiled=True)


def normalised(tokens, norm_gain, norm_shift):
    floats = tokens.astype(jnp.float32)
    own = jnp.stack([jnp.sum(floats, axis=1), jnp.sum(floats * floats, axis=1)])
    sums = own + swap_tp(own)
    full_width = tokens.shape[1] * lax.axis_size("tp")
    average = sums[0] / full_width
    variance = sums[1] / full_width - average * average
    return (
        (floats - average[:, None]) * lax.rsqrt(variance[:, None] + norm_eps) * norm_gain
        + norm_shift
    ).astype(jnp.bfloat16)


def expert_half(rows, gate_weight, up_weight, down_weight):
    gate_pre = jnp.dot(rows, gate_weight[0], preferred_element_type=jnp.float32)
    up_pre = jnp.dot(rows, up_weight[0], preferred_element_type=jnp.float32)
    gate_cut = jnp.minimum(gate_pre, clamp_limit)
    up_cut = jnp.clip(up_pre, -clamp_limit, clamp_limit)
    hidden = ((up_cut + 1.0) * gate_cut * jax.nn.sigmoid(sigmoid_slope * gate_cut)).astype(
        jnp.bfloat16
    )
    return jnp.dot(hidden, down_weight[0], preferred_element_type=jnp.float32).astype(jnp.bfloat16)


def body(tokens, routes, gate_logits, norm_gain, norm_shift, gate_weight, up_weight, down_weight):
    experts = lax.axis_size("ep")
    rows, top_count = routes.shape
    width = tokens.shape[1]
    capacity = rows * top_count // experts + 2
    half = lax.axis_index("tp")
    blocks = width // lanes
    slots = experts * capacity

    normed = normalised(tokens, norm_gain, norm_shift)
    exp_logits = jnp.exp(gate_logits)
    weights = exp_logits / jnp.sum(exp_logits, axis=1, keepdims=True)
    match = routes[:, :, None] == jnp.arange(experts, dtype=jnp.int32)[None, None, :]
    chosen = jnp.any(match, axis=1)
    weight_of = jnp.sum(jnp.where(match, weights[:, :, None], 0.0), axis=1)
    before = (jnp.arange(rows)[:, None] > jnp.arange(rows)[None, :]).astype(jnp.bfloat16)
    rank = jnp.dot(before, chosen.astype(jnp.bfloat16), preferred_element_type=jnp.float32)
    rank = jnp.where(chosen, rank, -1.0)
    places = jnp.arange(capacity, dtype=jnp.float32)
    taken = rank[:, :, None] == places[None, None, :]
    pick = taken.reshape(rows, slots).astype(jnp.bfloat16)
    packed = lax.dot_general(
        pick, normed, (((0,), (0,)), ((), ())), preferred_element_type=jnp.float32
    ).astype(jnp.bfloat16)
    arrived = exchange(packed.reshape(experts, capacity * blocks, lanes))
    other = swap_tp(arrived)
    own_rows = arrived.reshape(slots, width)
    other_rows = other.reshape(slots, width)
    first = jnp.where(half == 0, own_rows, other_rows)
    second = jnp.where(half == 0, other_rows, own_rows)
    partial_out = expert_half(
        jnp.concatenate([first, second], axis=1), gate_weight, up_weight, down_weight
    )
    low, high = (partial_out[:, :width], partial_out[:, width:])
    kept = jnp.where(half == 0, low, high).reshape(experts, capacity * blocks, lanes)
    given = jnp.where(half == 0, high, low).reshape(experts, capacity * blocks, lanes)
    got = swap_tp(given)
    answered = (kept.astype(jnp.float32) + got.astype(jnp.float32)).astype(jnp.bfloat16)
    returned = exchange(answered).reshape(slots, width)
    blend = jnp.where(taken, weight_of[:, :, None], 0.0).reshape(rows, slots)
    blend_high = blend.astype(jnp.bfloat16)
    blend_low = (blend - blend_high.astype(jnp.float32)).astype(jnp.bfloat16)
    mixed = jnp.dot(blend_high, returned, preferred_element_type=jnp.float32) + jnp.dot(
        blend_low, returned, preferred_element_type=jnp.float32
    )
    return mixed.astype(jnp.bfloat16)


def solution(mesh):
    placed = (
        P(("grp", "ep"), "tp"),
        P(("grp", "ep"), None),
        P(("grp", "ep"), None),
        P("tp"),
        P("tp"),
        P("ep", None, "tp"),
        P("ep", None, "tp"),
        P("ep", "tp", None),
    )
    return jax.shard_map(
        body, mesh=mesh, in_specs=placed, out_specs=P(("grp", "ep"), "tp"), check_vma=False
    )
```

time: 199 us -> 166 us (0.83)
  blocking collectives: 104 us -> 84.1 us
  waiting for transfers between devices: 63.9 us -> 54.9 us
  local copies, waits for them, and re-layouts: 11.4 us -> 4 us
  matrix products: 4.19 us -> 8.11 us
  starting transfers between devices: 9.03 us -> 6.08 us
  other arithmetic: 3.47 us -> 6.04 us
    all_to_all x3 -> x1, blocking collectives: 104 us -> 84.1 us  [exchange(): return lax.all_to_all(x, 'ep', split_axis=0, concat_axis=0, tiled=True)]
    all_to_all x2 -> x1, waiting for transfers between devices: 63.9 us -> 52.4 us  [exchange(): return lax.all_to_all(x, 'ep', split_axis=0, concat_axis=0, tiled=True)]
    dot_general x2 -> x6, matrix products: 4.19 us -> 8.11 us  [the longest x1 3.59 us: expert_half(): jnp.dot(hidden, down_weight[0], preferred_element_type=jnp.float32)]
    all_to_all x2 -> x1, starting transfers between devices: 9.03 us -> 5.8 us  [exchange(): return lax.all_to_all(x, 'ep', split_axis=0, concat_axis=0, tiled=True)]
    another operation x2 -> x0, local copies, waits for them, and re-layouts: 2.79 us -> none  [split_up(): return jnp.moveaxis(x.reshape(*before, length, -1, *after), dim, 0)]
    ppermute x0 -> x3, waiting for transfers between devices: none -> 2.52 us  [swap_tp(): return lax.ppermute(x, 'tp', [(0, 1), (1, 0)])]
    scatter x1 -> x0, local copies, waits for them, and re-layouts: 2.14 us -> none  [body(): outgoing = jnp.zeros((ep_count * capacity, send_width), jnp.bfloat16).at[...]
  transfers between devices with their start and end apart: 2 -> 4, of which waited for: 1 -> 3; matrix products, arithmetic and copies ran while one was open for 1% -> 1% of each run, Pallas kernels for 0% -> 0%
where the time goes in v1:
time: 166 us; the launch traced here: 163 us
  blocking collectives  84.1 us (51%)
  waiting for transfers between devices  54.9 us (33%)
  matrix products  8.11 us (5%)
  starting transfers between devices  6.08 us (4%)
  other arithmetic  6.04 us (4%)
  local copies, waits for them, and re-layouts  4 us (2%)
    all_to_all x1, blocking collectives, exchange(): return lax.all_to_all(x, 'ep', split_axis=0, concat_axis=0, tiled=True)  84.1 us
    all_to_all x1, waiting for transfers between devices, exchange(): return lax.all_to_all(x, 'ep', split_axis=0, concat_axis=0, tiled=True)  52.4 us
    all_to_all x1, starting transfers between devices, exchange(): return lax.all_to_all(x, 'ep', split_axis=0, concat_axis=0, tiled=True)  5.8 us
    dot_general x1, matrix products, expert_half(): jnp.dot(hidden, down_weight[0], preferred_element_type=jnp.float32)  3.59 us
  transfers between devices with their start and end apart: 4, of which 3 were waited for; matrix products, arithmetic and copies ran while one was open for 1% of the time, Pallas kernels for 0%

profile of v1, /device:TPU:166, one launch (start us, length us, event | category | flops | bytes accessed | tf_op | source)
XLA Modules:
  0.0 163.4 jit_solution(9204672809896991055)
XLA Ops:
  0.0 1.1 convert_reduce_fusion
  1.1 0.1 collective-permute-start
  1.3 0.8 fusion.47
  2.1 0.1 convolution_select_fusion
  2.5 1.2 convolution_convert_fusion.1
  3.6 0.2 reshape.121
  3.8 84.1 %all_to_all.10 = bf16[32,48,128]{2,1,0:T(8,128)(2,1)S(1)} all-to-all(bf16[32,48,128]{2,1,0:T(8,128)(2,1)S(1)} %reshape.121), channel_id=1, replica_groups=mesh['grp'=4,'ep'=32,'tp'=2] {'ep'}, dimensions={0} | all-to-all | bytes 786432 | tf_op jit(solution)/shard_map/all_to_all | solution.py:17
  87.9 1.7 %collective-permute-done.1 = bf16[32,48,128]{2,1,0:T(8,128)(2,1)S(1)} collective-permute-done((bf16[32,48,128]{2,1,0:T(8,128)(2,1)S(1)}, bf16[32,48,128]{2,1,0:T(8,128)(2,1)S(1)}, u32[]{:S(2)}, u32[]{:S(2)}) %collective-permute-start.1) | collective-permute-done | bytes 393248 | tf_op jit(solution)/shard_map/ppermute | solution.py:13
  89.6 0.8 broadcast_select_fusion
  90.4 0.2 select_n.61
  90.6 1.2 select_n.63
  91.8 2.2 %fusion.17 = f32[192,512]{1,0:T(8,128)S(1)} fusion(bf16[192,2048]{1,0:T(8,128)(2,1)S(1)} %constant_dynamic-update-slice_fusion, bf16[1,2048,512]{2,1,0:T(8,128)(2,1)} %param.13), kind=kOutput, calls=%fused_computation.11 | convolution fusion | flops 402751488 | bytes 3276800 | tf_op jit(solution)/shard_map/dot_general | solution.py:34
  94.0 3.6 %convolution_convert_fusion = bf16[192,2048]{1,0:T(8,128)(2,1)} fusion(bf16[1,512,2048]{2,1,0:T(8,128)(2,1)S(1)} %copy-done, f32[192,512]{1,0:T(8,128)S(1)} %fusion.17, bf16[192,2048]{1,0:T(8,128)(2,1)S(1)} %constant_dynamic-update-slice_fusion, bf16[1,2048,512]{2,1,0:T(8,128)(2,1)} %param.14), kind=kOutput, calls=%fused_computation | convolution fusion | flops 806584320 | bytes 6160384 | tf_op jit(solution)/shard_map/dot_general | solution.py:41
  97.6 1.2 broadcast_select_fusion.2
  98.8 0.9 reshape.122
  99.7 0.1 collective-permute-start.2
  99.9 1.0 reshape.124
  100.9 0.8 collective-permute-done.2
  101.7 2.0 %add_convert_fusion = bf16[32,48,128]{2,1,0:T(8,128)(2,1)} fusion(f32[32,48,128]{2,1,0:T(8,128)} %reshape.124, bf16[32,48,128]{2,1,0:T(8,128)(2,1)S(1)} %collective-permute-done.2), kind=kLoop, calls=%fused_computation.16 | loop fusion | flops 589824 | bytes 1572864 | tf_op jit(solution)/shard_map/convert_element_type | solution.py:81
  103.6 5.8 %all-to-all-start.1 = ((bf16[32,48,128]{2,1,0:T(8,128)(2,1)}), bf16[32,48,128]{2,1,0:T(8,128)(2,1)S(1)}, u32[]{:S(2)}, u32[]{:S(2)}) async-start(bf16[32,48,128]{2,1,0:T(8,128)(2,1)} %add_convert_fusion), calls=%async_computation.1 | async-start | bytes 786432 | tf_op jit(solution)/shard_map/all_to_all | solution.py:17
  109.8 52.4 %all-to-all-done.1 = bf16[32,48,128]{2,1,0:T(8,128)(2,1)S(1)} async-done(((bf16[32,48,128]{2,1,0:T(8,128)(2,1)}), bf16[32,48,128]{2,1,0:T(8,128)(2,1)S(1)}, u32[]{:S(2)}, u32[]{:S(2)}) %all-to-all-start.1) | async-done | bytes 393248 | tf_op jit(solution)/shard_map/all_to_all | solution.py:17
  162.2 0.2 reshape.123
  162.4 0.2 fusion.56
  162.6 0.9 fusion.25
  (27 shorter events, 0.6 us)
Async XLA Ops:
  0.0 94.0 %copy-start = (bf16[1,512,2048]{2,1,0:T(8,128)(2,1)S(1)}, bf16[1,512,2048]{2,1,0:T(8,128)(2,1)}, u32[]{:S(2)}) copy-start(bf16[1,512,2048]{2,1,0:T(8,128)(2,1)} %param.15) | copy-start | bytes 6291460
  1.1 1.3 collective-permute-start
  87.9 1.7 %collective-permute-start.1 = (bf16[32,48,128]{2,1,0:T(8,128)(2,1)S(1)}, bf16[32,48,128]{2,1,0:T(8,128)(2,1)S(1)}, u32[]{:S(2)}, u32[]{:S(2)}) collective-permute-start(bf16[32,48,128]{2,1,0:T(8,128)(2,1)S(1)} %all_to_all.10), channel_id=1, source_target_pairs={{0,1},{1,0},{2,3},{3,2},{4,5},{5,4},{6,7},{7,6},{8,9},{9,8},{10,11... | collective-permute-start | bytes 1179656 | tf_op jit(solution)/shard_map/ppermute | solution.py:13
  99.7 9.7 %copy-start.2 = (f32[32,4]{0,1:T(4,128)S(1)}, f32[32,4]{0,1:T(4,128)}, u32[]{:S(2)}) copy-start(f32[32,4]{0,1:T(4,128)} %param.10) | copy-start | bytes 1540
  99.7 9.7 %copy-start.1 = (s32[32,4]{0,1:T(4,128)S(1)}, s32[32,4]{0,1:T(4,128)}, u32[]{:S(2)}) copy-start(s32[32,4]{0,1:T(4,128)} %param.9) | copy-start | bytes 1540
  99.7 1.9 %collective-permute-start.2 = (bf16[32,48,128]{2,1,0:T(8,128)(2,1)}, bf16[32,48,128]{2,1,0:T(8,128)(2,1)S(1)}, u32[]{:S(2)}, u32[]{:S(2)}) collective-permute-start(bf16[32,48,128]{2,1,0:T(8,128)(2,1)} %reshape.122), channel_id=1, source_target_pairs={{0,1},{1,0},{2,3},{3,2},{4,5},{5,4},{6,7},{7,6},{8,9},{9,8},{10,11... | collective-permute-start | bytes 1179656 | tf_op jit(solution)/shard_map/ppermute | solution.py:13
  103.6 58.6 %all-to-all-start.1 = ((bf16[32,48,128]{2,1,0:T(8,128)(2,1)}), bf16[32,48,128]{2,1,0:T(8,128)(2,1)S(1)}, u32[]{:S(2)}, u32[]{:S(2)}) async-start(bf16[32,48,128]{2,1,0:T(8,128)(2,1)} %add_convert_fusion), calls=%async_computation.1 | async-start | bytes 786432 | tf_op jit(solution)/shard_map/all_to_all | solution.py:17

commit v2 on v1

v2 whole, which is shorter than its diff:
```python
import functools

import jax
import jax.numpy as jnp
from jax import lax
from jax.experimental import pallas as pl
from jax.experimental.pallas import tpu as pltpu
from jax.sharding import PartitionSpec as P

norm_eps = 1e-05
clamp_limit = 7.0
sigmoid_slope = 1.702
lanes = 128


def swap_tp(x):
    return lax.ppermute(x, "tp", [(0, 1), (1, 0)])


def exchange(x):
    return lax.all_to_all(x, "ep", split_axis=0, concat_axis=0, tiled=True)


def in_hbm(x):
    return pltpu.with_memory_space_constraint(x, pltpu.HBM)


def load_kernel(tokens_hbm, routes_hbm, logits_hbm, gain_hbm, shift_hbm, gate_hbm, sums_ref, tokens_ref, routes_ref, logits_ref, gain_ref, shift_ref, gate_ref, sems):
    pairs = (
        (tokens_hbm, tokens_ref),
        (routes_hbm, routes_ref),
        (logits_hbm, logits_ref),
        (gain_hbm, gain_ref),
        (shift_hbm, shift_ref),
        (gate_hbm, gate_ref),
    )
    copies = [pltpu.make_async_copy(*pair, sems.at[i]) for i, pair in enumerate(pairs)]
    for copy in copies:
        copy.start()
    copies[0].wait()
    rows, width = tokens_ref.shape
    total = jnp.zeros((rows, lanes), jnp.float32)
    squares = jnp.zeros((rows, lanes), jnp.float32)
    for j in range(width // lanes):
        part = tokens_ref[:, j * lanes : (j + 1) * lanes].astype(jnp.float32)
        total = total + part
        squares = squares + part * part
    sums_ref[:rows, :] = total
    sums_ref[rows:, :] = squares
    for copy in copies[1:]:
        copy.wait()


def plan_kernel(capacity, routes_ref, logits_ref, up_hbm, pick_ref, high_ref, low_ref, up_ref, sem):
    copy = pltpu.make_async_copy(up_hbm, up_ref, sem)
    copy.start()
    top_count, rows = routes_ref.shape
    slots = pick_ref.shape[0]
    experts = slots // capacity
    exp_logits = jnp.exp(logits_ref[...])
    weights = exp_logits / jnp.sum(exp_logits, axis=0, keepdims=True)
    expert_id = lax.broadcasted_iota(jnp.int32, (experts, rows), 0)
    chosen = jnp.zeros((experts, rows), jnp.float32)
    weight_of = jnp.zeros((experts, rows), jnp.float32)
    for k in range(top_count):
        match = routes_ref[k : k + 1, :] == expert_id
        chosen = jnp.where(match, 1.0, chosen)
        weight_of = jnp.where(match, weights[k : k + 1, :], weight_of)
    earlier = lax.broadcasted_iota(jnp.int32, (rows, rows), 0) < lax.broadcasted_iota(
        jnp.int32, (rows, rows), 1
    )
    rank = jnp.dot(
        chosen.astype(jnp.bfloat16),
        jnp.where(earlier, 1.0, 0.0).astype(jnp.bfloat16),
        preferred_element_type=jnp.float32,
    )
    slot_of = jnp.where(
        chosen > 0.0, rank + (expert_id * capacity).astype(jnp.float32), -1.0
    ).astype(jnp.bfloat16)
    slot_id = lax.broadcasted_iota(jnp.int32, (slots, experts), 0)
    first = lax.broadcasted_iota(jnp.int32, (slots, experts), 1) * capacity
    spread = jnp.where((slot_id >= first) & (slot_id < first + capacity), 1.0, 0.0).astype(
        jnp.bfloat16
    )

    def to_slots(x):
        return jnp.dot(spread, x, preferred_element_type=jnp.float32)

    taken = to_slots(slot_of) == lax.broadcasted_iota(jnp.int32, (slots, rows), 0).astype(jnp.float32)
    high = weight_of.astype(jnp.bfloat16)
    low = (weight_of - high.astype(jnp.float32)).astype(jnp.bfloat16)
    pick_ref[...] = jnp.where(taken, 1.0, 0.0).astype(jnp.bfloat16)
    high_ref[...] = jnp.where(taken, to_slots(high), 0.0).astype(jnp.bfloat16)
    low_ref[...] = jnp.where(taken, to_slots(low), 0.0).astype(jnp.bfloat16)
    copy.wait()


def pack_kernel(full_width, tokens_ref, own_ref, other_ref, gain_ref, shift_ref, pick_ref, down_hbm, packed_ref, down_ref, wide, sem):
    copy = pltpu.make_async_copy(down_hbm, down_ref, sem)
    copy.start()
    rows, width = tokens_ref.shape
    slots = pick_ref.shape[0]
    blocks = width // lanes
    sums = jnp.sum(own_ref[...] + other_ref[...], axis=1, keepdims=True)
    average = sums[:rows, :] / full_width
    variance = sums[rows:, :] / full_width - average * average
    inverse = lax.rsqrt(variance + norm_eps)
    normed = [
        (
            (tokens_ref[:, j * lanes : (j + 1) * lanes].astype(jnp.float32) - average)
            * inverse
            * gain_ref[j : j + 1, :]
            + shift_ref[j : j + 1, :]
        ).astype(jnp.bfloat16)
        for j in range(blocks)
    ]
    packed = jnp.dot(
        pick_ref[...], jnp.concatenate(normed, axis=1), preferred_element_type=jnp.float32
    )
    for j in range(blocks):
        wide[pl.ds(j, slots, stride=blocks), :] = packed[:, j * lanes : (j + 1) * lanes]
    packed_ref[...] = wide[...].astype(jnp.bfloat16)
    copy.wait()


def in_kernel(name, kernel, outs, scratch=(), kinds=None):
    vmem = pl.BlockSpec(memory_space=pltpu.VMEM)
    return pl.pallas_call(
        kernel,
        out_shape=tuple(jax.ShapeDtypeStruct(shape, dtype) for shape, dtype in outs),
        in_specs=[pl.BlockSpec(memory_space=kind) for kind in kinds],
        out_specs=tuple(vmem for _ in outs),
        scratch_shapes=list(scratch),
        compiler_params=pltpu.CompilerParams(vmem_limit_bytes=16 << 20),
        name=name,
    )


def expert_kernel(own_ref, other_ref, gate_ref, up_ref, down_ref, kept_ref, given_ref, wide, rows_own, rows_other, out_wide):
    slots, width = rows_own.shape
    blocks = width // lanes
    half = lax.axis_index("tp")
    for source, target in ((own_ref, rows_own), (other_ref, rows_other)):
        wide[...] = source[...].astype(jnp.float32)
        for j in range(blocks):
            target[:, j * lanes : (j + 1) * lanes] = wide[pl.ds(j, slots, stride=blocks), :].astype(
                jnp.bfloat16
            )
    here = pl.multiple_of(half * width, width)
    there = pl.multiple_of((1 - half) * width, width)

    def project(weight_ref):
        return jnp.dot(
            rows_own[...], weight_ref[0, pl.ds(here, width), :], preferred_element_type=jnp.float32
        ) + jnp.dot(
            rows_other[...], weight_ref[0, pl.ds(there, width), :], preferred_element_type=jnp.float32
        )

    gate_cut = jnp.minimum(project(gate_ref), clamp_limit)
    up_cut = jnp.clip(project(up_ref), -clamp_limit, clamp_limit)
    hidden = ((up_cut + 1.0) * gate_cut * jax.nn.sigmoid(sigmoid_slope * gate_cut)).astype(
        jnp.bfloat16
    )
    for side in range(2):
        part = jnp.dot(
            hidden, down_ref[0, :, side * width : (side + 1) * width], preferred_element_type=jnp.float32
        )
        base = jnp.where(half == side, 0, slots * blocks)
        for j in range(blocks):
            out_wide[pl.ds(base + j, slots, stride=blocks), :] = part[:, j * lanes : (j + 1) * lanes]
    kept_ref[...] = out_wide[: slots * blocks, :].astype(jnp.bfloat16)
    given_ref[...] = out_wide[slots * blocks :, :].astype(jnp.bfloat16)


def body(tokens, routes, gate_logits, norm_gain, norm_shift, gate_weight, up_weight, down_weight):
    experts = lax.axis_size("ep")
    rows, top_count = routes.shape
    width = tokens.shape[1]
    full_width = width * lax.axis_size("tp")
    capacity = rows * top_count // experts + 2
    blocks = width // lanes
    slots = experts * capacity
    wire = (experts, capacity * blocks, lanes)
    tiles = (slots * blocks, lanes)
    bf16, f32 = jnp.bfloat16, jnp.float32
    vmem = pltpu.VMEM

    inputs = (tokens, routes.T, gate_logits.T, norm_gain.reshape(blocks, lanes), norm_shift.reshape(blocks, lanes), gate_weight)
    sums, tokens, routes, gate_logits, norm_gain, norm_shift, gate_weight = in_kernel(
        "load",
        load_kernel,
        [((2 * rows, lanes), f32)] + [(x.shape, x.dtype) for x in inputs],
        scratch=[pltpu.SemaphoreType.DMA((len(inputs),))],
        kinds=[pltpu.HBM] * len(inputs),
    )(*(in_hbm(x) for x in inputs))
    other_sums = swap_tp(sums)
    pick, high, low, up_weight = in_kernel(
        "plan",
        functools.partial(plan_kernel, capacity),
        [((slots, rows), bf16)] * 3 + [(up_weight.shape, bf16)],
        scratch=[pltpu.SemaphoreType.DMA(())],
        kinds=[vmem] * 2 + [pltpu.HBM],
    )(routes, gate_logits, in_hbm(up_weight))
    packed, down_weight = in_kernel(
        "pack",
        functools.partial(pack_kernel, full_width),
        [(tiles, bf16), (down_weight.shape, bf16)],
        scratch=[pltpu.VMEM(tiles, f32), pltpu.SemaphoreType.DMA(())],
        kinds=[vmem] * 6 + [pltpu.HBM],
    )(tokens, sums, other_sums, norm_gain, norm_shift, pick, in_hbm(down_weight))
    arrived = exchange(packed.reshape(wire)).reshape(tiles)
    other = swap_tp(arrived)
    kept, given = in_kernel(
        "expert",
        expert_kernel,
        [(tiles, bf16)] * 2,
        scratch=[
            pltpu.VMEM(tiles, f32),
            pltpu.VMEM((slots, width), bf16),
            pltpu.VMEM((slots, width), bf16),
            pltpu.VMEM((2 * tiles[0], lanes), f32),
        ],
        kinds=[vmem] * 5,
    )(arrived, other, gate_weight, up_weight, down_weight)
    got = swap_tp(given)
    answered = (kept.astype(f32) + got.astype(f32)).astype(bf16)
    returned = exchange(answered.reshape(wire)).reshape(slots, width)

    def blended(blend):
        return lax.dot_general(
            blend, returned, (((0,), (0,)), ((), ())), preferred_element_type=f32
        )

    return (blended(high) + blended(low)).astype(bf16)


def solution(mesh):
    placed = (
        P(("grp", "ep"), "tp"),
        P(("grp", "ep"), None),
        P(("grp", "ep"), None),
        P("tp"),
        P("tp"),
        P("ep", None, "tp"),
        P("ep", None, "tp"),
        P("ep", "tp", None),
    )
    return jax.shard_map(
        body, mesh=mesh, in_specs=placed, out_specs=P(("grp", "ep"), "tp"), check_vma=False
    )
```

time: 166 us -> 156 us (0.940)
  blocking collectives: 84.1 us -> 142 us
  waiting for transfers between devices: 54.9 us -> 3.31 us
  matrix products: 8.11 us -> 1.05 us
  Pallas kernels: 0 us -> 6.97 us
  other arithmetic: 6.04 us -> 0.1 us
  starting transfers between devices: 6.08 us -> 0.4 us
  local copies, waits for them, and re-layouts: 4 us -> 0.17 us
    all_to_all x1 -> x2, blocking collectives: 84.1 us -> 142 us  [exchange(): return lax.all_to_all(x, 'ep', split_axis=0, concat_axis=0, tiled=True)]
    all_to_all x1 -> x0, waiting for transfers between devices: 52.4 us -> none  [exchange(): return lax.all_to_all(x, 'ep', split_axis=0, concat_axis=0, tiled=True)]
    dot_general x6 -> x2, matrix products: 8.11 us -> 1.05 us  [blended(): lax.dot_general(blend, returned, (((0,), (0,)), ((), ())), preferred_elem...]
    pallas_call x0 -> x4, Pallas kernels: none -> 6.97 us  [the longest x1 2.01 us: body(): in_kernel('expert', expert_kernel, [(tiles, bf16)] * 2, scratch=[pltpu.VM...]
    all_to_all x1 -> x0, starting transfers between devices: 5.8 us -> none  [exchange(): return lax.all_to_all(x, 'ep', split_axis=0, concat_axis=0, tiled=True)]
    select_n x2 -> x0, other arithmetic: 1.99 us -> none  [the longest x1 1.19 us: body(): jnp.where(half == 0, high, low).reshape(experts, capacity * blocks, lanes)]
    convert_element_type x3 -> x1, other arithmetic: 2.01 us -> 0.1 us  [body(): answered = (kept.astype(f32) + got.astype(f32)).astype(bf16)]
  transfers between devices with their start and end apart: 4 -> 3, of which waited for: 3 -> 2; matrix products, arithmetic and copies ran while one was open for 1% -> 0% of each run, Pallas kernels for 0% -> 1%
where the time goes in v2:
time: 156 us; the launch traced here: 154 us
  blocking collectives  142 us (91%)
  Pallas kernels  6.97 us (4%)
  waiting for transfers between devices  3.31 us (2%)
    all_to_all x2, blocking collectives, exchange(): return lax.all_to_all(x, 'ep', split_axis=0, concat_axis=0, tiled=True)  142 us
    ppermute x3, waiting for transfers between devices, swap_tp(): return lax.ppermute(x, 'tp', [(0, 1), (1, 0)])  3.31 us
  transfers between devices with their start and end apart: 3, of which 2 were waited for; matrix products, arithmetic and copies ran while one was open for 0% of the time, Pallas kernels for 1%

profile of v2, /device:TPU:166, one launch (start us, length us, event | category | flops | bytes accessed | tf_op | source)
XLA Modules:
  0.0 153.8 jit_solution(14819702947304062531)
XLA Ops:
  0.0 1.7 %load.1 = (f32[64,128]{1,0:T(8,128)S(1)}, bf16[32,1024]{1,0:T(8,128)(2,1)S(1)}, s32[4,32]{1,0:T(4,128)S(1)}, f32[4,32]{1,0:T(4,128)S(1)}, f32[8,128]{1,0:T(8,128...) custom-call(bf16[32,1024]{1,0:T(8,128)(2,1)} %tokens_hbm.1, s32[4,32]{1,0:T(4,128)} %bitcast.17, ...), custom_call_target="tpu_custom_call" | custom-call | tf_op jit(solution)/shard_map/load/pallas_call | solution.py:189
  1.8 0.1 collective-permute-start
  1.9 1.6 %plan.1 = (bf16[192,32]{1,0:T(8,128)(2,1)S(1)}, bf16[192,32]{1,0:T(8,128)(2,1)S(1)}, bf16[192,32]{1,0:T(8,128)(2,1)S(1)}, bf16[1,2048,512]{2,1,0:T(8,128)(2,1)S(1)}) custom-call(s32[4,32]{1,0:T(4,128)S(1)} %get-tuple-element.20.routes_ref, f32[4,32]{1,0:T(4,128)S(1)} %get-tuple-element.21.logits_ref, bf16[1,2048,512]{2,1,0:T(8,128)(2,1)} %up_hbm.1), custom_call_target="tpu_custom_call" | custom-call | tf_op jit(solution)/shard_map/plan/pallas_call | solution.py:197
  3.5 0.0 collective-permute-done.other_ref
  3.5 1.6 %pack.1 = (bf16[1536,128]{1,0:T(8,128)(2,1)S(1)}, bf16[1,512,2048]{2,1,0:T(8,128)(2,1)S(1)}) custom-call(bf16[32,1024]{1,0:T(8,128)(2,1)S(1)} %get-tuple-element.23.tokens_ref, f32[64,128]{1,0:T(8,128)S(1)} %get-tuple-element.24.own_ref, f32[64,128]{1,0:T(8,128)S(1)} %collective-permute-done.other_ref, f32[8,128]{1,0:T(8,128)S(1)} %get-tuple-element.25.gain_ref, ...), custom_call_target="tpu_custom_call" | custom-call | tf_op jit(solution)/shard_map/pack/pallas_call | solution.py:204
  5.1 84.1 %all_to_all.10 = bf16[32,48,128]{2,1,0:T(8,128)(2,1)S(1)} all-to-all(bf16[32,48,128]{2,1,0:T(8,128)(2,1)S(1)} %bitcast.13), channel_id=1, replica_groups=mesh['grp'=4,'ep'=32,'tp'=2] {'ep'}, dimensions={0} | all-to-all | bytes 786432 | tf_op jit(solution)/shard_map/all_to_all | solution.py:21
  89.2 0.0 collective-permute-start.1
  89.2 1.7 %collective-permute-done.1.other_ref = bf16[1536,128]{1,0:T(8,128)(2,1)S(1)} collective-permute-done((bf16[1536,128]{1,0:T(8,128)(2,1)S(1)}, bf16[1536,128]{1,0:T(8,128)(2,1)S(1)}, u32[]{:S(2)}, u32[]{:S(2)}) %collective-permute-start.1) | collective-permute-done | bytes 393248 | tf_op jit(solution)/shard_map/ppermute | solution.py:17
  91.0 2.0 %expert.1 = (bf16[1536,128]{1,0:T(8,128)(2,1)S(1)}, bf16[1536,128]{1,0:T(8,128)(2,1)S(1)}) custom-call(bf16[1536,128]{1,0:T(8,128)(2,1)S(1)} %bitcast.12, bf16[1536,128]{1,0:T(8,128)(2,1)S(1)} %collective-permute-done.1.other_ref, bf16[1,2048,512]{2,1,0:T(8,128)(2,1)S(1)} %get-tuple-element.29.gate_ref, bf16[1,2048,512]{2,1,0:T(8,128)(2,1)S(1)} %get-tuple-element.30.up_ref, ...), custom_call_target="tpu_custom_call" | custom-call | tf_op jit(solution)/shard_map/expert/pallas_call | solution.py:213
  93.0 0.3 collective-permute-start.2
  93.2 1.6 %collective-permute-done.2 = bf16[1536,128]{1,0:T(8,128)(2,1)S(1)} collective-permute-done((bf16[1536,128]{1,0:T(8,128)(2,1)S(1)}, bf16[1536,128]{1,0:T(8,128)(2,1)S(1)}, u32[]{:S(2)}, u32[]{:S(2)}) %collective-permute-start.2) | collective-permute-done | bytes 393248 | tf_op jit(solution)/shard_map/ppermute | solution.py:17
  94.8 0.1 add_convert_fusion
  94.9 57.7 %all_to_all.11 = bf16[32,48,128]{2,1,0:T(8,128)(2,1)S(1)} all-to-all(bf16[32,48,128]{2,1,0:T(8,128)(2,1)S(1)} %bitcast.14), channel_id=1, replica_groups=mesh['grp'=4,'ep'=32,'tp'=2] {'ep'}, dimensions={0} | all-to-all | bytes 786432 | tf_op jit(solution)/shard_map/all_to_all | solution.py:21
  152.6 0.2 reshape.23
  152.8 0.2 fusion.1
  153.0 0.9 fusion
Async XLA Ops:
  1.8 1.8 %collective-permute-start = (f32[64,128]{1,0:T(8,128)S(1)}, f32[64,128]{1,0:T(8,128)S(1)}, u32[]{:S(2)}, u32[]{:S(2)}) collective-permute-start(f32[64,128]{1,0:T(8,128)S(1)} %get-tuple-element.24.own_ref), channel_id=1, source_target_pairs={{0,1},{1,0},{2,3},{3,2},{4,5},{5,4},{6,7},{7,6},{8,9},{9,8},{10,11... | collective-permute-start | bytes 98312 | tf_op jit(solution)/shard_map/ppermute | solution.py:17
  89.2 1.7 %collective-permute-start.1 = (bf16[1536,128]{1,0:T(8,128)(2,1)S(1)}, bf16[1536,128]{1,0:T(8,128)(2,1)S(1)}, u32[]{:S(2)}, u32[]{:S(2)}) collective-permute-start(bf16[1536,128]{1,0:T(8,128)(2,1)S(1)} %bitcast.11), channel_id=1, source_target_pairs={{0,1},{1,0},{2,3},{3,2},{4,5},{5,4},{6,7},{7,6},{8,9},{9,8},{10,11... | collective-permute-start | bytes 1179656 | tf_op jit(solution)/shard_map/ppermute | solution.py:17
  93.0 1.8 %collective-permute-start.2 = (bf16[1536,128]{1,0:T(8,128)(2,1)S(1)}, bf16[1536,128]{1,0:T(8,128)(2,1)S(1)}, u32[]{:S(2)}, u32[]{:S(2)}) collective-permute-start(bf16[1536,128]{1,0:T(8,128)(2,1)S(1)} %get-tuple-element.33), channel_id=1, source_target_pairs={{0,1},{1,0},{2,3},{3,2},{4,5},{5,4},{6,7},{7,6},{8,9},{9,8},{10,11... | collective-permute-start | bytes 1179656 | tf_op jit(solution)/shard_map/ppermute | solution.py:17

commit v3 on v1

v3 whole, which is shorter than its diff:
```python
import functools

import jax
import jax.numpy as jnp
from jax import lax
from jax.experimental import pallas as pl
from jax.experimental.pallas import tpu as pltpu
from jax.sharding import PartitionSpec as P

norm_eps = 1e-05
clamp_limit = 7.0
sigmoid_slope = 1.702
lanes = 128


def swap_tp(x):
    return lax.ppermute(x, "tp", [(0, 1), (1, 0)])


def exchange(x):
    return lax.all_to_all(x, "ep", split_axis=0, concat_axis=0, tiled=True)


def in_kernel(name, kernel, outs, scratch, kinds):
    vmem = pl.BlockSpec(memory_space=pltpu.VMEM)
    return pl.pallas_call(
        kernel,
        out_shape=tuple(jax.ShapeDtypeStruct(shape, dtype) for shape, dtype in outs),
        in_specs=[pl.BlockSpec(memory_space=kind) for kind in kinds],
        out_specs=tuple(vmem for _ in outs),
        scratch_shapes=list(scratch),
        compiler_params=pltpu.CompilerParams(vmem_limit_bytes=16 << 20),
        name=name,
    )


def in_hbm(x):
    return pltpu.with_memory_space_constraint(x, pltpu.HBM)


def start_all(pairs, sems):
    copies = [pltpu.make_async_copy(*pair, sems.at[i]) for i, pair in enumerate(pairs)]
    for copy in copies:
        copy.start()
    return copies


def pack_kernel(capacity, routes_hbm, logits_hbm, tokens_hbm, gain_hbm, shift_hbm, gate_hbm, packed_ref, high_ref, low_ref, affine_ref, gate_ref, routes_ref, logits_ref, tokens_ref, wide, sems):
    top_count, rows = routes_ref.shape
    slots = high_ref.shape[0]
    experts = slots // capacity
    blocks = tokens_ref.shape[1] // lanes
    copies = start_all(
        (
            (routes_hbm, routes_ref),
            (logits_hbm, logits_ref),
            (tokens_hbm, tokens_ref),
            (gain_hbm, affine_ref.at[0:blocks]),
            (shift_hbm, affine_ref.at[blocks : 2 * blocks]),
            (gate_hbm, gate_ref),
        ),
        sems,
    )
    copies[0].wait()
    expert_id = lax.broadcasted_iota(jnp.int32, (experts, rows), 0)
    matches = [routes_ref[k : k + 1, :] == expert_id for k in range(top_count)]
    chosen = functools.reduce(jnp.logical_or, matches)
    earlier = lax.broadcasted_iota(jnp.int32, (rows, rows), 0) < lax.broadcasted_iota(
        jnp.int32, (rows, rows), 1
    )
    rank = jnp.dot(
        jnp.where(chosen, 1.0, 0.0).astype(jnp.bfloat16),
        jnp.where(earlier, 1.0, 0.0).astype(jnp.bfloat16),
        preferred_element_type=jnp.float32,
    )
    slot_of = jnp.where(
        chosen, rank + (expert_id * capacity).astype(jnp.float32), -1.0
    ).astype(jnp.bfloat16)
    slot_id = lax.broadcasted_iota(jnp.int32, (slots, experts), 0)
    first = lax.broadcasted_iota(jnp.int32, (slots, experts), 1) * capacity
    spread = jnp.where((slot_id >= first) & (slot_id < first + capacity), 1.0, 0.0).astype(
        jnp.bfloat16
    )

    def to_slots(x):
        return jnp.dot(spread, x, preferred_element_type=jnp.float32)

    taken = to_slots(slot_of) == lax.broadcasted_iota(jnp.int32, (slots, rows), 0).astype(jnp.float32)
    pick = jnp.where(taken, 1.0, 0.0).astype(jnp.bfloat16)
    copies[2].wait()
    packed = jnp.dot(pick, tokens_ref[...], preferred_element_type=jnp.float32)
    for j in range(blocks):
        wide[pl.ds(j, slots, stride=blocks), :] = packed[:, j * lanes : (j + 1) * lanes]
    packed_ref[...] = wide[...].astype(jnp.bfloat16)
    copies[1].wait()
    exp_logits = jnp.exp(logits_ref[...])
    weights = exp_logits / jnp.sum(exp_logits, axis=0, keepdims=True)
    weight_of = jnp.zeros((experts, rows), jnp.float32)
    for k, match in enumerate(matches):
        weight_of = jnp.where(match, weights[k : k + 1, :], weight_of)
    high = weight_of.astype(jnp.bfloat16)
    low = (weight_of - high.astype(jnp.float32)).astype(jnp.bfloat16)
    high_ref[...] = jnp.where(taken, to_slots(high), 0.0).astype(jnp.bfloat16)
    low_ref[...] = jnp.where(taken, to_slots(low), 0.0).astype(jnp.bfloat16)
    for copy in copies[3:]:
        copy.wait()


def unpack(tiles_ref, rows_ref, sums_ref, wide):
    slots, width = rows_ref.shape
    blocks = width // lanes
    wide[...] = tiles_ref[...].astype(jnp.float32)
    total = jnp.zeros((slots, lanes), jnp.float32)
    squares = jnp.zeros((slots, lanes), jnp.float32)
    for j in range(blocks):
        part = wide[pl.ds(j, slots, stride=blocks), :]
        rows_ref[:, j * lanes : (j + 1) * lanes] = part.astype(jnp.bfloat16)
        total = total + part
        squares = squares + part * part
    sums_ref[:slots, :] = total
    sums_ref[slots:, :] = squares


def own_kernel(own_ref, up_hbm, rows_ref, sums_ref, up_ref, wide, sems):
    copies = start_all(((up_hbm, up_ref),), sems)
    unpack(own_ref, rows_ref, sums_ref, wide)
    copies[0].wait()


def give(part, wide, out_ref):
    slots = part.shape[0]
    blocks = part.shape[1] // lanes
    for j in range(blocks):
        wide[pl.ds(j, slots, stride=blocks), :] = part[:, j * lanes : (j + 1) * lanes]
    out_ref[...] = wide[...].astype(jnp.bfloat16)


def expert_kernel(rows_own, own_sums, other_ref, own_affine, other_affine, gate_ref, up_ref, down_hbm, hidden_ref, given_ref, wide, rows_other, other_sums, down_ref, sems):
    slots, width = rows_own.shape
    blocks = width // lanes
    half = lax.axis_index("tp")
    here = pl.multiple_of(half * width, width)
    there = pl.multiple_of((1 - half) * width, width)
    copies = start_all(((down_hbm.at[0, :, pl.ds(there, width)], down_ref),), sems)
    unpack(other_ref, rows_other, other_sums, wide)
    sums = jnp.sum(own_sums[...] + other_sums[...], axis=1, keepdims=True)
    average = sums[:slots, :] / (2 * width)
    variance = sums[slots:, :] / (2 * width) - average * average
    inverse = lax.rsqrt(variance + norm_eps)

    def normalised(rows_ref, affine_ref):
        return jnp.concatenate(
            [
                (
                    (rows_ref[:, j * lanes : (j + 1) * lanes].astype(jnp.float32) - average)
                    * inverse
                    * affine_ref[j : j + 1, :]
                    + affine_ref[blocks + j : blocks + j + 1, :]
                ).astype(jnp.bfloat16)
                for j in range(blocks)
            ],
            axis=1,
        )

    own = normalised(rows_own, own_affine)
    other = normalised(rows_other, other_affine)

    def project(weight_ref):
        return jnp.dot(
            own, weight_ref[0, pl.ds(here, width), :], preferred_element_type=jnp.float32
        ) + jnp.dot(
            other, weight_ref[0, pl.ds(there, width), :], preferred_element_type=jnp.float32
        )

    gate_cut = jnp.minimum(project(gate_ref), clamp_limit)
    up_cut = jnp.clip(project(up_ref), -clamp_limit, clamp_limit)
    hidden = ((up_cut + 1.0) * gate_cut * jax.nn.sigmoid(sigmoid_slope * gate_cut)).astype(
        jnp.bfloat16
    )
    hidden_ref[...] = hidden
    copies[0].wait()
    give(jnp.dot(hidden, down_ref[...], preferred_element_type=jnp.float32), wide, given_ref)


def kept_kernel(hidden_ref, down_hbm, kept_ref, wide, down_ref, sems):
    width = down_ref.shape[1]
    here = pl.multiple_of(lax.axis_index("tp") * width, width)
    copies = start_all(((down_hbm.at[0, :, pl.ds(here, width)], down_ref),), sems)
    copies[0].wait()
    give(jnp.dot(hidden_ref[...], down_ref[...], preferred_element_type=jnp.float32), wide, kept_ref)


def body(tokens, routes, gate_logits, norm_gain, norm_shift, gate_weight, up_weight, down_weight):
    experts = lax.axis_size("ep")
    rows, top_count = routes.shape
    width = tokens.shape[1]
    capacity = rows * top_count // experts + 2
    blocks = width // lanes
    slots = experts * capacity
    wire = (experts, capacity * blocks, lanes)
    tiles = (slots * blocks, lanes)
    bf16, f32 = jnp.bfloat16, jnp.float32
    vmem, hbm = pltpu.VMEM, pltpu.HBM

    packed, high, low, affine, gate_weight = in_kernel(
        "pack",
        functools.partial(pack_kernel, capacity),
        [
            (tiles, bf16),
            ((slots, rows), bf16),
            ((slots, rows), bf16),
            ((2 * blocks, lanes), f32),
            (gate_weight.shape, bf16),
        ],
        scratch=[
            pltpu.VMEM((top_count, rows), jnp.int32),
            pltpu.VMEM((top_count, rows), f32),
            pltpu.VMEM(tokens.shape, bf16),
            pltpu.VMEM(tiles, f32),
            pltpu.SemaphoreType.DMA((6,)),
        ],
        kinds=[hbm] * 6,
    )(
        in_hbm(routes.T),
        in_hbm(gate_logits.T),
        in_hbm(tokens),
        in_hbm(norm_gain.reshape(blocks, lanes)),
        in_hbm(norm_shift.reshape(blocks, lanes)),
        in_hbm(gate_weight),
    )
    arrived = exchange(packed.reshape(wire)).reshape(tiles)
    arrived, affine = lax.optimization_barrier((arrived, affine))
    other = swap_tp(arrived)
    other_affine = swap_tp(affine)
    rows_own, own_sums, up_weight = in_kernel(
        "own",
        own_kernel,
        [((slots, width), bf16), ((2 * slots, lanes), f32), (up_weight.shape, bf16)],
        scratch=[pltpu.VMEM(tiles, f32), pltpu.SemaphoreType.DMA((1,))],
        kinds=[vmem, hbm],
    )(arrived, in_hbm(up_weight))
    down_half = pltpu.VMEM((down_weight.shape[1], width), bf16)
    hidden, given = in_kernel(
        "expert",
        expert_kernel,
        [((slots, gate_weight.shape[2]), bf16), (tiles, bf16)],
        scratch=[
            pltpu.VMEM(tiles, f32),
            pltpu.VMEM((slots, width), bf16),
            pltpu.VMEM((2 * slots, lanes), f32),
            down_half,
            pltpu.SemaphoreType.DMA((1,)),
        ],
        kinds=[vmem] * 7 + [hbm],
    )(rows_own, own_sums, other, affine, other_affine, gate_weight, up_weight, in_hbm(down_weight))
    (kept,) = in_kernel(
        "kept",
        kept_kernel,
        [(tiles, bf16)],
        scratch=[pltpu.VMEM(tiles, f32), down_half, pltpu.SemaphoreType.DMA((1,))],
        kinds=[vmem, hbm],
    )(hidden, in_hbm(down_weight))
    got = swap_tp(given)
    answered = (kept.astype(f32) + got.astype(f32)).astype(bf16)
    returned = exchange(answered.reshape(wire)).reshape(slots, width)

    def blended(blend):
        return lax.dot_general(
            blend, returned, (((0,), (0,)), ((), ())), preferred_element_type=f32
        )

    return (blended(high) + blended(low)).astype(bf16)


def solution(mesh):
    placed = (
        P(("grp", "ep"), "tp"),
        P(("grp", "ep"), None),
        P(("grp", "ep"), None),
        P("tp"),
        P("tp"),
        P("ep", None, "tp"),
        P("ep", None, "tp"),
        P("ep", "tp", None),
    )
    return jax.shard_map(
        body, mesh=mesh, in_specs=placed, out_specs=P(("grp", "ep"), "tp"), check_vma=False
    )
```

time: 166 us -> 154 us (0.928)
  blocking collectives: 84.1 us -> 142 us
  waiting for transfers between devices: 54.9 us -> 0.02 us
  Pallas kernels: 0 us -> 7.53 us
  matrix products: 8.11 us -> 1.05 us
  other arithmetic: 6.04 us -> 0.1 us
  starting transfers between devices: 6.08 us -> 0.65 us
  local copies, waits for them, and re-layouts: 4 us -> 0.17 us
    all_to_all x1 -> x2, blocking collectives: 84.1 us -> 142 us  [exchange(): return lax.all_to_all(x, 'ep', split_axis=0, concat_axis=0, tiled=True)]
    all_to_all x1 -> x0, waiting for transfers between devices: 52.4 us -> none  [exchange(): return lax.all_to_all(x, 'ep', split_axis=0, concat_axis=0, tiled=True)]
    pallas_call x0 -> x4, Pallas kernels: none -> 7.53 us  [the longest x1 2.51 us: body(): in_kernel('expert', expert_kernel, [((slots, gate_weight.shape[2]), bf16)...]
    dot_general x6 -> x2, matrix products: 8.11 us -> 1.05 us  [blended(): lax.dot_general(blend, returned, (((0,), (0,)), ((), ())), preferred_elem...]
    all_to_all x1 -> x0, starting transfers between devices: 5.8 us -> none  [exchange(): return lax.all_to_all(x, 'ep', split_axis=0, concat_axis=0, tiled=True)]
    ppermute x3, waiting for transfers between devices: 2.52 us -> 0.02 us  [swap_tp(): return lax.ppermute(x, 'tp', [(0, 1), (1, 0)])]
    select_n x2 -> x0, other arithmetic: 1.99 us -> none  [the longest x1 1.19 us: body(): jnp.where(half == 0, high, low).reshape(experts, capacity * blocks, lanes)]
    convert_element_type x3 -> x1, other arithmetic: 2.01 us -> 0.1 us  [body(): answered = (kept.astype(f32) + got.astype(f32)).astype(bf16)]
  transfers between devices with their start and end apart: 4 -> 3, of which waited for: 3 -> 0; matrix products, arithmetic and copies ran while one was open for 1% -> 0% of each run, Pallas kernels for 0% -> 2%
where the time goes in v3:
time: 154 us; the launch traced here: 151 us
  blocking collectives  142 us (92%)
  Pallas kernels  7.53 us (5%)
    all_to_all x2, blocking collectives, exchange(): return lax.all_to_all(x, 'ep', split_axis=0, concat_axis=0, tiled=True)  142 us
  transfers between devices with their start and end apart: 3, of which 0 were waited for; matrix products, arithmetic and copies ran while one was open for 0% of the time, Pallas kernels for 2%

profile of v3, /device:TPU:166, one launch (start us, length us, event | category | flops | bytes accessed | tf_op | source)
XLA Modules:
  0.0 151.2 jit_solution(13680484218532223778)
XLA Ops:
  0.0 1.7 %pack.1 = (bf16[1536,128]{1,0:T(8,128)(2,1)S(1)}, bf16[192,32]{1,0:T(8,128)(2,1)S(1)}, bf16[192,32]{1,0:T(8,128)(2,1)S(1)}, f32[16,128]{1,0:T(8,128)S(1)}, bf16[1,2048,512]{2,1,0:T(8,128)(2,1)S(1)}) custom-call(s32[4,32]{1,0:T(4,128)} %bitcast.17, f32[4,32]{1,0:T(4,128)} %bitcast.18, bf16[32,1024]{1,0:T(8,128)(2,1)} %tokens_hbm.1, f32[8,128]{1,0:T(8,128)} %bitcast.15, ...), custom_call_target="tpu_custom_call" | custom-call | tf_op jit(solution)/shard_map/pack/pallas_call | solution.py:205
  1.8 83.6 %all_to_all.10 = bf16[32,48,128]{2,1,0:T(8,128)(2,1)S(1)} all-to-all(bf16[32,48,128]{2,1,0:T(8,128)(2,1)S(1)} %bitcast.13), channel_id=1, replica_groups=mesh['grp'=4,'ep'=32,'tp'=2] {'ep'}, dimensions={0} | all-to-all | bytes 786432 | tf_op jit(solution)/shard_map/all_to_all | solution.py:21
  85.4 0.0 collective-permute-start
  85.4 0.5 collective-permute-start.1
  85.9 1.6 %own.1 = (bf16[192,1024]{1,0:T(8,128)(2,1)S(1)}, f32[384,128]{1,0:T(8,128)S(1)}, bf16[1,2048,512]{2,1,0:T(8,128)(2,1)S(1)}) custom-call(bf16[1536,128]{1,0:T(8,128)(2,1)S(1)} %bitcast.12, bf16[1,2048,512]{2,1,0:T(8,128)(2,1)} %up_hbm.1), custom_call_target="tpu_custom_call" | custom-call | tf_op jit(solution)/shard_map/own/pallas_call | solution.py:235
  87.5 0.0 collective-permute-done.1.other_affine
  87.5 0.0 collective-permute-done.other_ref
  87.5 2.5 %expert.1 = (bf16[192,512]{1,0:T(8,128)(2,1)S(1)}, bf16[1536,128]{1,0:T(8,128)(2,1)S(1)}) custom-call(bf16[192,1024]{1,0:T(8,128)(2,1)S(1)} %get-tuple-element.21.rows_own, f32[384,128]{1,0:T(8,128)S(1)} %get-tuple-element.22.own_sums, bf16[1536,128]{1,0:T(8,128)(2,1)S(1)} %collective-permute-done.other_ref, f32[16,128]{1,0:T(8,128)S(1)} %get-tuple-element.23.own_affine, ...), custom_call_target="tpu_custom_call" | custom-call | tf_op jit(solution)/shard_map/expert/pallas_call | solution.py:243
  90.0 0.1 collective-permute-start.2
  90.2 1.7 %kept.1 = bf16[1536,128]{1,0:T(8,128)(2,1)S(1)} custom-call(bf16[192,512]{1,0:T(8,128)(2,1)S(1)} %get-tuple-element.26.hidden_ref, bf16[1,512,2048]{2,1,0:T(8,128)(2,1)} %down_hbm.3), custom_call_target="tpu_custom_call" | custom-call | tf_op jit(solution)/shard_map/kept/pallas_call | solution.py:256
  91.8 0.0 collective-permute-done.2
  91.9 0.1 add_convert_fusion
  92.0 58.0 %all_to_all.11 = bf16[32,48,128]{2,1,0:T(8,128)(2,1)S(1)} all-to-all(bf16[32,48,128]{2,1,0:T(8,128)(2,1)S(1)} %bitcast.14), channel_id=1, replica_groups=mesh['grp'=4,'ep'=32,'tp'=2] {'ep'}, dimensions={0} | all-to-all | bytes 786432 | tf_op jit(solution)/shard_map/all_to_all | solution.py:21
  150.0 0.2 reshape.23
  150.2 0.2 fusion.1
  150.4 0.9 fusion
Async XLA Ops:
  85.4 2.1 %collective-permute-start = (bf16[1536,128]{1,0:T(8,128)(2,1)S(1)}, bf16[1536,128]{1,0:T(8,128)(2,1)S(1)}, u32[]{:S(2)}, u32[]{:S(2)}) collective-permute-start(bf16[1536,128]{1,0:T(8,128)(2,1)S(1)} %bitcast.11), channel_id=1, source_target_pairs={{0,1},{1,0},{2,3},{3,2},{4,5},{5,4},{6,7},{7,6},{8,9},{9,8},{10,11... | collective-permute-start | bytes 1179656 | tf_op jit(solution)/shard_map/ppermute | solution.py:17
  85.4 2.1 %collective-permute-start.1 = (f32[16,128]{1,0:T(8,128)S(1)}, f32[16,128]{1,0:T(8,128)S(1)}, u32[]{:S(2)}, u32[]{:S(2)}) collective-permute-start(f32[16,128]{1,0:T(8,128)S(1)} %get-tuple-element.23.own_affine), channel_id=1, source_target_pairs={{0,1},{1,0},{2,3},{3,2},{4,5},{5,4},{6,7},{7,6},{8,9},{9,8},{10,11... | collective-permute-start | bytes 24584 | tf_op jit(solution)/shard_map/ppermute | solution.py:17
  90.0 1.8 %collective-permute-start.2 = (bf16[1536,128]{1,0:T(8,128)(2,1)S(1)}, bf16[1536,128]{1,0:T(8,128)(2,1)S(1)}, u32[]{:S(2)}, u32[]{:S(2)}) collective-permute-start(bf16[1536,128]{1,0:T(8,128)(2,1)S(1)} %get-tuple-element.27), channel_id=1, source_target_pairs={{0,1},{1,0},{2,3},{3,2},{4,5},{5,4},{6,7},{7,6},{8,9},{9,8},{10,11... | collective-permute-start | bytes 1179656 | tf_op jit(solution)/shard_map/ppermute | solution.py:17

commit v4 on v3

--- a/solution.py
+++ b/solution.py
@@ -17,8 +17,15 @@
     return lax.ppermute(x, "tp", [(0, 1), (1, 0)])
 
 
+def ring_order():
+    count = lax.axis_size("ep")
+    return [(3 * count // 4 + k) % count for k in range(count)]
+
+
 def exchange(x):
-    return lax.all_to_all(x, "ep", split_axis=0, concat_axis=0, tiled=True)
+    return lax.all_to_all(
+        x, "ep", split_axis=0, concat_axis=0, axis_index_groups=[ring_order()], tiled=True
+    )
 
 
 def in_kernel(name, kernel, outs, scratch, kinds):
@@ -45,7 +52,7 @@
     return copies
 
 
-def pack_kernel(capacity, routes_hbm, logits_hbm, tokens_hbm, gain_hbm, shift_hbm, gate_hbm, packed_ref, high_ref, low_ref, affine_ref, gate_ref, routes_ref, logits_ref, tokens_ref, wide, sems):
+def pack_kernel(capacity, first_expert, routes_hbm, logits_hbm, tokens_hbm, gain_hbm, shift_hbm, gate_hbm, packed_ref, high_ref, low_ref, affine_ref, gate_ref, routes_ref, logits_ref, tokens_ref, wide, sems):
     top_count, rows = routes_ref.shape
     slots = high_ref.shape[0]
     experts = slots // capacity
@@ -62,7 +69,8 @@
         sems,
     )
     copies[0].wait()
-    expert_id = lax.broadcasted_iota(jnp.int32, (experts, rows), 0)
+    expert_id = (lax.broadcasted_iota(jnp.int32, (experts, rows), 0) + first_expert) % experts
+    place = lax.broadcasted_iota(jnp.int32, (experts, rows), 0) * capacity
     matches = [routes_ref[k : k + 1, :] == expert_id for k in range(top_count)]
     chosen = functools.reduce(jnp.logical_or, matches)
     earlier = lax.broadcasted_iota(jnp.int32, (rows, rows), 0) < lax.broadcasted_iota(
@@ -74,7 +82,7 @@
         preferred_element_type=jnp.float32,
     )
     slot_of = jnp.where(
-        chosen, rank + (expert_id * capacity).astype(jnp.float32), -1.0
+        chosen, rank + place.astype(jnp.float32), -1.0
     ).astype(jnp.bfloat16)
     slot_id = lax.broadcasted_iota(jnp.int32, (slots, experts), 0)
     first = lax.broadcasted_iota(jnp.int32, (slots, experts), 1) * capacity
@@ -204,7 +212,7 @@
 
     packed, high, low, affine, gate_weight = in_kernel(
         "pack",
-        functools.partial(pack_kernel, capacity),
+        functools.partial(pack_kernel, capacity, ring_order()[0]),
         [
             (tiles, bf16),
             ((slots, rows), bf16),

time: 154 us -> 143 us (0.929); the launches traced: 151 us -> 143 us
  blocking collectives: 142 us -> 133 us
    all_to_all x2, blocking collectives: 142 us -> 133 us  [exchange(): lax.all_to_all(x, 'ep', split_axis=0, concat_axis=0, axis_index_groups=[r...]
where the time goes in v4:
time: 143 us
  blocking collectives  133 us (93%)
  Pallas kernels  7.53 us (5%)
    all_to_all x2, blocking collectives, exchange(): lax.all_to_all(x, 'ep', split_axis=0, concat_axis=0, axis_index_groups=[r...  133 us
  transfers between devices with their start and end apart: 3, of which 0 were waited for; matrix products, arithmetic and copies ran while one was open for 0% of the time, Pallas kernels for 2%

profile of v4, /device:TPU:166, one launch (start us, length us, event | category | flops | bytes accessed | tf_op | source)
XLA Modules:
  0.0 142.6 jit_solution(17459025570749667881)
XLA Ops:
  0.0 1.7 %pack.1 = (bf16[1536,128]{1,0:T(8,128)(2,1)S(1)}, bf16[192,32]{1,0:T(8,128)(2,1)S(1)}, bf16[192,32]{1,0:T(8,128)(2,1)S(1)}, f32[16,128]{1,0:T(8,128)S(1)}, bf16[1,2048,512]{2,1,0:T(8,128)(2,1)S(1)}) custom-call(s32[4,32]{1,0:T(4,128)} %bitcast.17, f32[4,32]{1,0:T(4,128)} %bitcast.18, bf16[32,1024]{1,0:T(8,128)(2,1)} %tokens_hbm.1, f32[8,128]{1,0:T(8,128)} %bitcast.15, ...), custom_call_target="tpu_custom_call" | custom-call | tf_op jit(solution)/shard_map/pack/pallas_call | solution.py:213
  1.8 75.0 %all_to_all.10 = bf16[32,48,128]{2,1,0:T(8,128)(2,1)S(1)} all-to-all(bf16[32,48,128]{2,1,0:T(8,128)(2,1)S(1)} %bitcast.13), channel_id=1, replica_groups={{48,50,52,54,56,58,60,62,0,2,4,6,8,10,12,14,16,18,20,22,24,26,28,30,32,..., dimensions={0} | all-to-all | bytes 786432 | tf_op jit(solution)/shard_map/all_to_all | solution.py:26
  76.7 0.0 collective-permute-start
  76.7 0.5 collective-permute-start.1
  77.2 1.6 %own.1 = (bf16[192,1024]{1,0:T(8,128)(2,1)S(1)}, f32[384,128]{1,0:T(8,128)S(1)}, bf16[1,2048,512]{2,1,0:T(8,128)(2,1)S(1)}) custom-call(bf16[1536,128]{1,0:T(8,128)(2,1)S(1)} %bitcast.12, bf16[1,2048,512]{2,1,0:T(8,128)(2,1)} %up_hbm.1), custom_call_target="tpu_custom_call" | custom-call | tf_op jit(solution)/shard_map/own/pallas_call | solution.py:243
  78.8 0.0 collective-permute-done.1.other_affine
  78.8 0.0 collective-permute-done.other_ref
  78.9 2.5 %expert.1 = (bf16[192,512]{1,0:T(8,128)(2,1)S(1)}, bf16[1536,128]{1,0:T(8,128)(2,1)S(1)}) custom-call(bf16[192,1024]{1,0:T(8,128)(2,1)S(1)} %get-tuple-element.21.rows_own, f32[384,128]{1,0:T(8,128)S(1)} %get-tuple-element.22.own_sums, bf16[1536,128]{1,0:T(8,128)(2,1)S(1)} %collective-permute-done.other_ref, f32[16,128]{1,0:T(8,128)S(1)} %get-tuple-element.23.own_affine, ...), custom_call_target="tpu_custom_call" | custom-call | tf_op jit(solution)/shard_map/expert/pallas_call | solution.py:251
  81.4 0.1 collective-permute-start.2
  81.5 1.7 %kept.1 = bf16[1536,128]{1,0:T(8,128)(2,1)S(1)} custom-call(bf16[192,512]{1,0:T(8,128)(2,1)S(1)} %get-tuple-element.26.hidden_ref, bf16[1,512,2048]{2,1,0:T(8,128)(2,1)} %down_hbm.3), custom_call_target="tpu_custom_call" | custom-call | tf_op jit(solution)/shard_map/kept/pallas_call | solution.py:264
  83.2 0.0 collective-permute-done.2
  83.2 0.1 add_convert_fusion
  83.3 58.0 %all_to_all.11 = bf16[32,48,128]{2,1,0:T(8,128)(2,1)S(1)} all-to-all(bf16[32,48,128]{2,1,0:T(8,128)(2,1)S(1)} %bitcast.14), channel_id=1, replica_groups={{48,50,52,54,56,58,60,62,0,2,4,6,8,10,12,14,16,18,20,22,24,26,28,30,32,..., dimensions={0} | all-to-all | bytes 786432 | tf_op jit(solution)/shard_map/all_to_all | solution.py:26
  141.3 0.2 reshape.23
  141.5 0.2 fusion.1
  141.7 0.9 fusion
Async XLA Ops:
  76.7 2.1 %collective-permute-start = (bf16[1536,128]{1,0:T(8,128)(2,1)S(1)}, bf16[1536,128]{1,0:T(8,128)(2,1)S(1)}, u32[]{:S(2)}, u32[]{:S(2)}) collective-permute-start(bf16[1536,128]{1,0:T(8,128)(2,1)S(1)} %bitcast.11), channel_id=1, source_target_pairs={{0,1},{1,0},{2,3},{3,2},{4,5},{5,4},{6,7},{7,6},{8,9},{9,8},{10,11... | collective-permute-start | bytes 1179656 | tf_op jit(solution)/shard_map/ppermute | solution.py:17
  76.7 2.1 %collective-permute-start.1 = (f32[16,128]{1,0:T(8,128)S(1)}, f32[16,128]{1,0:T(8,128)S(1)}, u32[]{:S(2)}, u32[]{:S(2)}) collective-permute-start(f32[16,128]{1,0:T(8,128)S(1)} %get-tuple-element.23.own_affine), channel_id=1, source_target_pairs={{0,1},{1,0},{2,3},{3,2},{4,5},{5,4},{6,7},{7,6},{8,9},{9,8},{10,11... | collective-permute-start | bytes 24584 | tf_op jit(solution)/shard_map/ppermute | solution.py:17
  81.4 1.8 %collective-permute-start.2 = (bf16[1536,128]{1,0:T(8,128)(2,1)S(1)}, bf16[1536,128]{1,0:T(8,128)(2,1)S(1)}, u32[]{:S(2)}, u32[]{:S(2)}) collective-permute-start(bf16[1536,128]{1,0:T(8,128)(2,1)S(1)} %get-tuple-element.27), channel_id=1, source_target_pairs={{0,1},{1,0},{2,3},{3,2},{4,5},{5,4},{6,7},{7,6},{8,9},{9,8},{10,11... | collective-permute-start | bytes 1179656 | tf_op jit(solution)/shard_map/ppermute | solution.py:17

commit v5 on v4

--- a/solution.py
+++ b/solution.py
@@ -52,9 +52,21 @@
     return copies
 
 
-def pack_kernel(capacity, first_expert, routes_hbm, logits_hbm, tokens_hbm, gain_hbm, shift_hbm, gate_hbm, packed_ref, high_ref, low_ref, affine_ref, gate_ref, routes_ref, logits_ref, tokens_ref, wide, sems):
+def expert_ids(experts, rows, first_expert):
+    return (lax.broadcasted_iota(jnp.int32, (experts, rows), 0) + first_expert) % experts
+
+
+def spread_of(slots, experts, capacity):
+    slot_id = lax.broadcasted_iota(jnp.int32, (slots, experts), 0)
+    first = lax.broadcasted_iota(jnp.int32, (slots, experts), 1) * capacity
+    return jnp.where((slot_id >= first) & (slot_id < first + capacity), 1.0, 0.0).astype(
+        jnp.bfloat16
+    )
+
+
+def pack_kernel(capacity, first_expert, routes_hbm, logits_hbm, tokens_hbm, gain_hbm, shift_hbm, gate_hbm, packed_ref, pick_ref, affine_ref, gate_ref, routes_ref, logits_ref, tokens_ref, wide, sems):
     top_count, rows = routes_ref.shape
-    slots = high_ref.shape[0]
+    slots = pick_ref.shape[0]
     experts = slots // capacity
     blocks = tokens_ref.shape[1] // lanes
     copies = start_all(
@@ -69,7 +81,7 @@
         sems,
     )
     copies[0].wait()
-    expert_id = (lax.broadcasted_iota(jnp.int32, (experts, rows), 0) + first_expert) % experts
+    expert_id = expert_ids(experts, rows, first_expert)
     place = lax.broadcasted_iota(jnp.int32, (experts, rows), 0) * capacity
     matches = [routes_ref[k : k + 1, :] == expert_id for k in range(top_count)]
     chosen = functools.reduce(jnp.logical_or, matches)
@@ -84,32 +96,17 @@
     slot_of = jnp.where(
         chosen, rank + place.astype(jnp.float32), -1.0
     ).astype(jnp.bfloat16)
-    slot_id = lax.broadcasted_iota(jnp.int32, (slots, experts), 0)
-    first = lax.broadcasted_iota(jnp.int32, (slots, experts), 1) * capacity
-    spread = jnp.where((slot_id >= first) & (slot_id < first + capacity), 1.0, 0.0).astype(
-        jnp.bfloat16
-    )
-
-    def to_slots(x):
-        return jnp.dot(spread, x, preferred_element_type=jnp.float32)
-
-    taken = to_slots(slot_of) == lax.broadcasted_iota(jnp.int32, (slots, rows), 0).astype(jnp.float32)
+    spread = spread_of(slots, experts, capacity)
+    at_slots = jnp.dot(spread, slot_of, preferred_element_type=jnp.float32)
+    taken = at_slots == lax.broadcasted_iota(jnp.int32, (slots, rows), 0).astype(jnp.float32)
     pick = jnp.where(taken, 1.0, 0.0).astype(jnp.bfloat16)
+    pick_ref[...] = pick
     copies[2].wait()
     packed = jnp.dot(pick, tokens_ref[...], preferred_element_type=jnp.float32)
     for j in range(blocks):
         wide[pl.ds(j, slots, stride=blocks), :] = packed[:, j * lanes : (j + 1) * lanes]
     packed_ref[...] = wide[...].astype(jnp.bfloat16)
     copies[1].wait()
-    exp_logits = jnp.exp(logits_ref[...])
-    weights = exp_logits / jnp.sum(exp_logits, axis=0, keepdims=True)
-    weight_of = jnp.zeros((experts, rows), jnp.float32)
-    for k, match in enumerate(matches):
-        weight_of = jnp.where(match, weights[k : k + 1, :], weight_of)
-    high = weight_of.astype(jnp.bfloat16)
-    low = (weight_of - high.astype(jnp.float32)).astype(jnp.bfloat16)
-    high_ref[...] = jnp.where(taken, to_slots(high), 0.0).astype(jnp.bfloat16)
-    low_ref[...] = jnp.where(taken, to_slots(low), 0.0).astype(jnp.bfloat16)
     for copy in copies[3:]:
         copy.wait()
 
@@ -143,18 +140,25 @@
     out_ref[...] = wide[...].astype(jnp.bfloat16)
 
 
-def expert_kernel(rows_own, own_sums, other_ref, own_affine, other_affine, gate_ref, up_ref, down_hbm, hidden_ref, given_ref, wide, rows_other, other_sums, down_ref, sems):
+def expert_kernel(rows_own, own_sums, other_ref, own_affine, other_affine, gate_ref, up_ref, down_hbm, hidden_ref, given_ref, down_kept, wide, rows_other, other_sums, down_given, sems):
     slots, width = rows_own.shape
     blocks = width // lanes
     half = lax.axis_index("tp")
     here = pl.multiple_of(half * width, width)
     there = pl.multiple_of((1 - half) * width, width)
-    copies = start_all(((down_hbm.at[0, :, pl.ds(there, width)], down_ref),), sems)
+    copies = start_all(
+        (
+            (down_hbm.at[0, :, pl.ds(there, width)], down_given),
+            (down_hbm.at[0, :, pl.ds(here, width)], down_kept),
+        ),
+        sems,
+    )
     unpack(other_ref, rows_other, other_sums, wide)
     sums = jnp.sum(own_sums[...] + other_sums[...], axis=1, keepdims=True)
     average = sums[:slots, :] / (2 * width)
     variance = sums[slots:, :] / (2 * width) - average * average
-    inverse = lax.rsqrt(variance + norm_eps)
+    inverse = jnp.broadcast_to(lax.rsqrt(variance + norm_eps), (slots, lanes))
+    average = jnp.broadcast_to(average, (slots, lanes))
 
     def normalised(rows_ref, affine_ref):
         return jnp.concatenate(
@@ -187,15 +191,28 @@
     )
     hidden_ref[...] = hidden
     copies[0].wait()
-    give(jnp.dot(hidden, down_ref[...], preferred_element_type=jnp.float32), wide, given_ref)
-
-
-def kept_kernel(hidden_ref, down_hbm, kept_ref, wide, down_ref, sems):
-    width = down_ref.shape[1]
-    here = pl.multiple_of(lax.axis_index("tp") * width, width)
-    copies = start_all(((down_hbm.at[0, :, pl.ds(here, width)], down_ref),), sems)
-    copies[0].wait()
+    give(jnp.dot(hidden, down_given[...], preferred_element_type=jnp.float32), wide, given_ref)
+    copies[1].wait()
+
+
+def kept_kernel(capacity, first_expert, hidden_ref, down_ref, routes_ref, logits_ref, pick_ref, kept_ref, high_ref, low_ref, wide):
     give(jnp.dot(hidden_ref[...], down_ref[...], preferred_element_type=jnp.float32), wide, kept_ref)
+    top_count, rows = routes_ref.shape
+    slots = pick_ref.shape[0]
+    experts = slots // capacity
+    exp_logits = jnp.exp(logits_ref[...])
+    weights = exp_logits / jnp.sum(exp_logits, axis=0, keepdims=True)
+    expert_id = expert_ids(experts, rows, first_expert)
+    weight_of = jnp.zeros((experts, rows), jnp.float32)
+    for k in range(top_count):
+        weight_of = jnp.where(routes_ref[k : k + 1, :] == expert_id, weights[k : k + 1, :], weight_of)
+    high = weight_of.astype(jnp.bfloat16)
+    low = (weight_of - high.astype(jnp.float32)).astype(jnp.bfloat16)
+    spread = spread_of(slots, experts, capacity)
+    taken = pick_ref[...].astype(jnp.float32) > 0.0
+    for part, part_ref in ((high, high_ref), (low, low_ref)):
+        at_slots = jnp.dot(spread, part, preferred_element_type=jnp.float32)
+        part_ref[...] = jnp.where(taken, at_slots, 0.0).astype(jnp.bfloat16)
 
 
 def body(tokens, routes, gate_logits, norm_gain, norm_shift, gate_weight, up_weight, down_weight):
@@ -210,19 +227,18 @@
     bf16, f32 = jnp.bfloat16, jnp.float32
     vmem, hbm = pltpu.VMEM, pltpu.HBM
 
-    packed, high, low, affine, gate_weight = in_kernel(
+    packed, pick, affine, gate_weight, routes, gate_logits = in_kernel(
         "pack",
         functools.partial(pack_kernel, capacity, ring_order()[0]),
         [
             (tiles, bf16),
             ((slots, rows), bf16),
-            ((slots, rows), bf16),
             ((2 * blocks, lanes), f32),
             (gate_weight.shape, bf16),
+            ((top_count, rows), jnp.int32),
+            ((top_count, rows), f32),
         ],
         scratch=[
-            pltpu.VMEM((top_count, rows), jnp.int32),
-            pltpu.VMEM((top_count, rows), f32),
             pltpu.VMEM(tokens.shape, bf16),
             pltpu.VMEM(tiles, f32),
             pltpu.SemaphoreType.DMA((6,)),
@@ -247,27 +263,27 @@
         scratch=[pltpu.VMEM(tiles, f32), pltpu.SemaphoreType.DMA((1,))],
         kinds=[vmem, hbm],
     )(arrived, in_hbm(up_weight))
-    down_half = pltpu.VMEM((down_weight.shape[1], width), bf16)
-    hidden, given = in_kernel(
+    down_half = (down_weight.shape[1], width)
+    hidden, given, down_kept = in_kernel(
         "expert",
         expert_kernel,
-        [((slots, gate_weight.shape[2]), bf16), (tiles, bf16)],
+        [((slots, gate_weight.shape[2]), bf16), (tiles, bf16), (down_half, bf16)],
         scratch=[
             pltpu.VMEM(tiles, f32),
             pltpu.VMEM((slots, width), bf16),
             pltpu.VMEM((2 * slots, lanes), f32),
-            down_half,
-            pltpu.SemaphoreType.DMA((1,)),
+            pltpu.VMEM(down_half, bf16),
+            pltpu.SemaphoreType.DMA((2,)),
         ],
         kinds=[vmem] * 7 + [hbm],
     )(rows_own, own_sums, other, affine, other_affine, gate_weight, up_weight, in_hbm(down_weight))
-    (kept,) = in_kernel(
+    kept, high, low = in_kernel(
         "kept",
-        kept_kernel,
-        [(tiles, bf16)],
-        scratch=[pltpu.VMEM(tiles, f32), down_half, pltpu.SemaphoreType.DMA((1,))],
-        kinds=[vmem, hbm],
-    )(hidden, in_hbm(down_weight))
+        functools.partial(kept_kernel, capacity, ring_order()[0]),
+        [(tiles, bf16), ((slots, rows), bf16), ((slots, rows), bf16)],
+        scratch=[pltpu.VMEM(tiles, f32)],
+        kinds=[vmem] * 5,
+    )(hidden, down_kept, routes, gate_logits, pick)
     got = swap_tp(given)
     answered = (kept.astype(f32) + got.astype(f32)).astype(bf16)
     returned = exchange(answered.reshape(wire)).reshape(slots, width)

time: 143 us -> 143 us (level)
  transfers between devices with their start and end apart: 3 -> 3, of which waited for: 0 -> 1; matrix products, arithmetic and copies ran while one was open for 0% -> 0% of each run, Pallas kernels for 2% -> 1%
where the time goes in v5:
time: 143 us; the launch traced here: 142 us
  blocking collectives  133 us (93%)
  Pallas kernels  6.31 us (4%)
    all_to_all x2, blocking collectives, exchange(): lax.all_to_all(x, 'ep', split_axis=0, concat_axis=0, axis_index_groups=[r...  133 us
  transfers between devices with their start and end apart: 3, of which 1 were waited for; matrix products, arithmetic and copies ran while one was open for 0% of the time, Pallas kernels for 1%

profile of v5, /device:TPU:166, one launch (start us, length us, event | category | flops | bytes accessed | tf_op | source)
XLA Modules:
  0.0 142.3 jit_solution(1452832803444183510)
XLA Ops:
  0.0 1.7 %pack.1 = (bf16[1536,128]{1,0:T(8,128)(2,1)S(1)}, bf16[192,32]{1,0:T(8,128)(2,1)S(1)}, f32[16,128]{1,0:T(8,128)S(1)}, bf16[1,2048,512]{2,1,0:T(8,128)(2,1)S(1)},...) custom-call(s32[4,32]{1,0:T(4,128)} %bitcast.17, f32[4,32]{1,0:T(4,128)} %bitcast.18, bf16[32,1024]{1,0:T(8,128)(2,1)} %tokens_hbm.1, ...), custom_call_target="tpu_custom_call" | custom-call | tf_op jit(solution)/shard_map/pack/pallas_call | solution.py:230
  1.8 75.0 %all_to_all.10 = bf16[32,48,128]{2,1,0:T(8,128)(2,1)S(1)} all-to-all(bf16[32,48,128]{2,1,0:T(8,128)(2,1)S(1)} %bitcast.13), channel_id=1, replica_groups={{48,50,52,54,56,58,60,62,0,2,4,6,8,10,12,14,16,18,20,22,24,26,28,30,32,..., dimensions={0} | all-to-all | bytes 786432 | tf_op jit(solution)/shard_map/all_to_all | solution.py:26
  76.7 0.0 collective-permute-start
  76.7 0.5 collective-permute-start.1
  77.2 1.6 %own.1 = (bf16[192,1024]{1,0:T(8,128)(2,1)S(1)}, f32[384,128]{1,0:T(8,128)S(1)}, bf16[1,2048,512]{2,1,0:T(8,128)(2,1)S(1)}) custom-call(bf16[1536,128]{1,0:T(8,128)(2,1)S(1)} %bitcast.12, bf16[1,2048,512]{2,1,0:T(8,128)(2,1)} %up_hbm.1), custom_call_target="tpu_custom_call" | custom-call | tf_op jit(solution)/shard_map/own/pallas_call | solution.py:259
  78.8 0.0 collective-permute-done.1.other_affine
  78.8 0.0 collective-permute-done.other_ref
  78.9 2.5 %expert.1 = (bf16[192,512]{1,0:T(8,128)(2,1)S(1)}, bf16[1536,128]{1,0:T(8,128)(2,1)S(1)}, bf16[512,1024]{1,0:T(8,128)(2,1)S(1)}) custom-call(bf16[192,1024]{1,0:T(8,128)(2,1)S(1)} %get-tuple-element.25.rows_own, f32[384,128]{1,0:T(8,128)S(1)} %get-tuple-element.26.own_sums, bf16[1536,128]{1,0:T(8,128)(2,1)S(1)} %collective-permute-done.other_ref, ...), custom_call_target="tpu_custom_call" | custom-call | tf_op jit(solution)/shard_map/expert/pallas_call | solution.py:267
  81.4 0.1 collective-permute-start.2
  81.5 0.5 kept.1
  82.0 1.2 collective-permute-done.2
  83.2 0.1 add_convert_fusion
  83.3 57.7 %all_to_all.11 = bf16[32,48,128]{2,1,0:T(8,128)(2,1)S(1)} all-to-all(bf16[32,48,128]{2,1,0:T(8,128)(2,1)S(1)} %bitcast.14), channel_id=1, replica_groups={{48,50,52,54,56,58,60,62,0,2,4,6,8,10,12,14,16,18,20,22,24,26,28,30,32,..., dimensions={0} | all-to-all | bytes 786432 | tf_op jit(solution)/shard_map/all_to_all | solution.py:26
  141.0 0.2 reshape.23
  141.2 0.2 fusion.1
  141.4 0.9 fusion
Async XLA Ops:
  76.7 2.1 %collective-permute-start = (bf16[1536,128]{1,0:T(8,128)(2,1)S(1)}, bf16[1536,128]{1,0:T(8,128)(2,1)S(1)}, u32[]{:S(2)}, u32[]{:S(2)}) collective-permute-start(bf16[1536,128]{1,0:T(8,128)(2,1)S(1)} %bitcast.11), channel_id=1, source_target_pairs={{0,1},{1,0},{2,3},{3,2},{4,5},{5,4},{6,7},{7,6},{8,9},{9,8},{10,11... | collective-permute-start | bytes 1179656 | tf_op jit(solution)/shard_map/ppermute | solution.py:17
  76.7 2.1 %collective-permute-start.1 = (f32[16,128]{1,0:T(8,128)S(1)}, f32[16,128]{1,0:T(8,128)S(1)}, u32[]{:S(2)}, u32[]{:S(2)}) collective-permute-start(f32[16,128]{1,0:T(8,128)S(1)} %get-tuple-element.27.own_affine), channel_id=1, source_target_pairs={{0,1},{1,0},{2,3},{3,2},{4,5},{5,4},{6,7},{7,6},{8,9},{9,8},{10,11... | collective-permute-start | bytes 24584 | tf_op jit(solution)/shard_map/ppermute | solution.py:17
  81.4 1.8 %collective-permute-start.2 = (bf16[1536,128]{1,0:T(8,128)(2,1)S(1)}, bf16[1536,128]{1,0:T(8,128)(2,1)S(1)}, u32[]{:S(2)}, u32[]{:S(2)}) collective-permute-start(bf16[1536,128]{1,0:T(8,128)(2,1)S(1)} %get-tuple-element.37), channel_id=1, source_target_pairs={{0,1},{1,0},{2,3},{3,2},{4,5},{5,4},{6,7},{7,6},{8,9},{9,8},{10,11... | collective-permute-start | bytes 1179656 | tf_op jit(solution)/shard_map/ppermute | solution.py:17

commit v6 on v5

--- a/solution.py
+++ b/solution.py
@@ -68,7 +68,9 @@
     top_count, rows = routes_ref.shape
     slots = pick_ref.shape[0]
     experts = slots // capacity
-    blocks = tokens_ref.shape[1] // lanes
+    width = tokens_ref.shape[1]
+    blocks = width // lanes
+    here = pl.multiple_of(lax.axis_index("tp") * width, width)
     copies = start_all(
         (
             (routes_hbm, routes_ref),
@@ -76,7 +78,7 @@
             (tokens_hbm, tokens_ref),
             (gain_hbm, affine_ref.at[0:blocks]),
             (shift_hbm, affine_ref.at[blocks : 2 * blocks]),
-            (gate_hbm, gate_ref),
+            (gate_hbm.at[0, pl.ds(here, width), :], gate_ref),
         ),
         sems,
     )
@@ -140,7 +142,7 @@
     out_ref[...] = wide[...].astype(jnp.bfloat16)
 
 
-def expert_kernel(rows_own, own_sums, other_ref, own_affine, other_affine, gate_ref, up_ref, down_hbm, hidden_ref, given_ref, down_kept, wide, rows_other, other_sums, down_given, sems):
+def expert_kernel(rows_own, own_sums, other_ref, own_affine, other_affine, gate_own, up_ref, gate_hbm, down_hbm, hidden_ref, given_ref, down_kept, wide, rows_other, other_sums, gate_other, down_given, sems):
     slots, width = rows_own.shape
     blocks = width // lanes
     half = lax.axis_index("tp")
@@ -148,6 +150,7 @@
     there = pl.multiple_of((1 - half) * width, width)
     copies = start_all(
         (
+            (gate_hbm.at[0, pl.ds(there, width), :], gate_other),
             (down_hbm.at[0, :, pl.ds(there, width)], down_given),
             (down_hbm.at[0, :, pl.ds(here, width)], down_kept),
         ),
@@ -177,22 +180,22 @@
     own = normalised(rows_own, own_affine)
     other = normalised(rows_other, other_affine)
 
-    def project(weight_ref):
-        return jnp.dot(
-            own, weight_ref[0, pl.ds(here, width), :], preferred_element_type=jnp.float32
-        ) + jnp.dot(
-            other, weight_ref[0, pl.ds(there, width), :], preferred_element_type=jnp.float32
+    def project(own_weight, other_weight):
+        return jnp.dot(own, own_weight, preferred_element_type=jnp.float32) + jnp.dot(
+            other, other_weight, preferred_element_type=jnp.float32
         )
 
-    gate_cut = jnp.minimum(project(gate_ref), clamp_limit)
-    up_cut = jnp.clip(project(up_ref), -clamp_limit, clamp_limit)
+    up_pre = project(up_ref[0, pl.ds(here, width), :], up_ref[0, pl.ds(there, width), :])
+    up_cut = jnp.clip(up_pre, -clamp_limit, clamp_limit)
+    copies[0].wait()
+    gate_cut = jnp.minimum(project(gate_own[...], gate_other[...]), clamp_limit)
     hidden = ((up_cut + 1.0) * gate_cut * jax.nn.sigmoid(sigmoid_slope * gate_cut)).astype(
         jnp.bfloat16
     )
     hidden_ref[...] = hidden
-    copies[0].wait()
+    copies[1].wait()
     give(jnp.dot(hidden, down_given[...], preferred_element_type=jnp.float32), wide, given_ref)
-    copies[1].wait()
+    copies[2].wait()
 
 
 def kept_kernel(capacity, first_expert, hidden_ref, down_ref, routes_ref, logits_ref, pick_ref, kept_ref, high_ref, low_ref, wide):
@@ -227,14 +230,15 @@
     bf16, f32 = jnp.bfloat16, jnp.float32
     vmem, hbm = pltpu.VMEM, pltpu.HBM
 
-    packed, pick, affine, gate_weight, routes, gate_logits = in_kernel(
+    gate_half = (width, gate_weight.shape[2])
+    packed, pick, affine, gate_own, routes, gate_logits = in_kernel(
         "pack",
         functools.partial(pack_kernel, capacity, ring_order()[0]),
         [
             (tiles, bf16),
             ((slots, rows), bf16),
             ((2 * blocks, lanes), f32),
-            (gate_weight.shape, bf16),
+            (gate_half, bf16),
             ((top_count, rows), jnp.int32),
             ((top_count, rows), f32),
         ],
@@ -272,11 +276,22 @@
             pltpu.VMEM(tiles, f32),
             pltpu.VMEM((slots, width), bf16),
             pltpu.VMEM((2 * slots, lanes), f32),
+            pltpu.VMEM(gate_half, bf16),
             pltpu.VMEM(down_half, bf16),
-            pltpu.SemaphoreType.DMA((2,)),
+            pltpu.SemaphoreType.DMA((3,)),
         ],
-        kinds=[vmem] * 7 + [hbm],
-    )(rows_own, own_sums, other, affine, other_affine, gate_weight, up_weight, in_hbm(down_weight))
+        kinds=[vmem] * 7 + [hbm] * 2,
+    )(
+        rows_own,
+        own_sums,
+        other,
+        affine,
+        other_affine,
+        gate_own,
+        up_weight,
+        in_hbm(gate_weight),
+        in_hbm(down_weight),
+    )
     kept, high, low = in_kernel(
         "kept",
         functools.partial(kept_kernel, capacity, ring_order()[0]),

time: 143 us -> 143 us (level)
  no operation moved by 1% of the time
where the time goes in v6:
time: 143 us; the launch traced here: 142 us
  blocking collectives  133 us (93%)
  Pallas kernels  6.42 us (4%)
    all_to_all x2, blocking collectives, exchange(): lax.all_to_all(x, 'ep', split_axis=0, concat_axis=0, axis_index_groups=[r...  133 us
    pallas_call x1, Pallas kernels, body(): in_kernel('expert', expert_kernel, [((slots, gate_weight.shape[2]), bf16)...  2.99 us
  transfers between devices with their start and end apart: 3, of which 1 were waited for; matrix products, arithmetic and copies ran while one was open for 0% of the time, Pallas kernels for 1%

profile of v6, /device:TPU:166, one launch (start us, length us, event | category | flops | bytes accessed | tf_op | source)
XLA Modules:
  0.0 142.4 jit_solution(10753747069814072255)
XLA Ops:
  0.0 1.4 pack.1
  1.4 75.0 %all_to_all.10 = bf16[32,48,128]{2,1,0:T(8,128)(2,1)S(1)} all-to-all(bf16[32,48,128]{2,1,0:T(8,128)(2,1)S(1)} %bitcast.13), channel_id=1, replica_groups={{48,50,52,54,56,58,60,62,0,2,4,6,8,10,12,14,16,18,20,22,24,26,28,30,32,..., dimensions={0} | all-to-all | bytes 786432 | tf_op jit(solution)/shard_map/all_to_all | solution.py:26
  76.3 0.0 collective-permute-start
  76.4 0.5 collective-permute-start.1
  76.9 1.6 %own.1 = (bf16[192,1024]{1,0:T(8,128)(2,1)S(1)}, f32[384,128]{1,0:T(8,128)S(1)}, bf16[1,2048,512]{2,1,0:T(8,128)(2,1)S(1)}) custom-call(bf16[1536,128]{1,0:T(8,128)(2,1)S(1)} %bitcast.12, bf16[1,2048,512]{2,1,0:T(8,128)(2,1)} %up_hbm.1), custom_call_target="tpu_custom_call" | custom-call | tf_op jit(solution)/shard_map/own/pallas_call | solution.py:263
  78.5 0.0 collective-permute-done.1.other_affine
  78.5 0.0 collective-permute-done.other_ref
  78.5 3.0 %expert.1 = (bf16[192,512]{1,0:T(8,128)(2,1)S(1)}, bf16[1536,128]{1,0:T(8,128)(2,1)S(1)}, bf16[512,1024]{1,0:T(8,128)(2,1)S(1)}) custom-call(bf16[192,1024]{1,0:T(8,128)(2,1)S(1)} %get-tuple-element.25.rows_own, f32[384,128]{1,0:T(8,128)S(1)} %get-tuple-element.26.own_sums, bf16[1536,128]{1,0:T(8,128)(2,1)S(1)} %collective-permute-done.other_ref, ...), custom_call_target="tpu_custom_call" | custom-call | tf_op jit(solution)/shard_map/expert/pallas_call | solution.py:271
  81.5 0.1 collective-permute-start.2
  81.6 0.5 kept.1
  82.1 1.2 collective-permute-done.2
  83.3 0.1 add_convert_fusion
  83.4 57.7 %all_to_all.11 = bf16[32,48,128]{2,1,0:T(8,128)(2,1)S(1)} all-to-all(bf16[32,48,128]{2,1,0:T(8,128)(2,1)S(1)} %bitcast.14), channel_id=1, replica_groups={{48,50,52,54,56,58,60,62,0,2,4,6,8,10,12,14,16,18,20,22,24,26,28,30,32,..., dimensions={0} | all-to-all | bytes 786432 | tf_op jit(solution)/shard_map/all_to_all | solution.py:26
  141.1 0.2 reshape.23
  141.3 0.2 fusion.1
  141.5 0.9 fusion
Async XLA Ops:
  76.3 2.1 %collective-permute-start = (bf16[1536,128]{1,0:T(8,128)(2,1)S(1)}, bf16[1536,128]{1,0:T(8,128)(2,1)S(1)}, u32[]{:S(2)}, u32[]{:S(2)}) collective-permute-start(bf16[1536,128]{1,0:T(8,128)(2,1)S(1)} %bitcast.11), channel_id=1, source_target_pairs={{0,1},{1,0},{2,3},{3,2},{4,5},{5,4},{6,7},{7,6},{8,9},{9,8},{10,11... | collective-permute-start | bytes 1179656 | tf_op jit(solution)/shard_map/ppermute | solution.py:17
  76.4 2.1 %collective-permute-start.1 = (f32[16,128]{1,0:T(8,128)S(1)}, f32[16,128]{1,0:T(8,128)S(1)}, u32[]{:S(2)}, u32[]{:S(2)}) collective-permute-start(f32[16,128]{1,0:T(8,128)S(1)} %get-tuple-element.27.own_affine), channel_id=1, source_target_pairs={{0,1},{1,0},{2,3},{3,2},{4,5},{5,4},{6,7},{7,6},{8,9},{9,8},{10,11... | collective-permute-start | bytes 24584 | tf_op jit(solution)/shard_map/ppermute | solution.py:17
  81.5 1.8 %collective-permute-start.2 = (bf16[1536,128]{1,0:T(8,128)(2,1)S(1)}, bf16[1536,128]{1,0:T(8,128)(2,1)S(1)}, u32[]{:S(2)}, u32[]{:S(2)}) collective-permute-start(bf16[1536,128]{1,0:T(8,128)(2,1)S(1)} %get-tuple-element.37), channel_id=1, source_target_pairs={{0,1},{1,0},{2,3},{3,2},{4,5},{5,4},{6,7},{7,6},{8,9},{9,8},{10,11... | collective-permute-start | bytes 1179656 | tf_op jit(solution)/shard_map/ppermute | solution.py:17

commit v7 on v5

--- a/solution.py
+++ b/solution.py
@@ -41,6 +41,10 @@
     )
 
 
+def in_vmem(x):
+    return pltpu.with_memory_space_constraint(x, pltpu.VMEM)
+
+
 def in_hbm(x):
     return pltpu.with_memory_space_constraint(x, pltpu.HBM)
 
@@ -64,7 +68,7 @@
     )
 
 
-def pack_kernel(capacity, first_expert, routes_hbm, logits_hbm, tokens_hbm, gain_hbm, shift_hbm, gate_hbm, packed_ref, pick_ref, affine_ref, gate_ref, routes_ref, logits_ref, tokens_ref, wide, sems):
+def pack_kernel(capacity, first_expert, routes_hbm, logits_hbm, tokens_hbm, gain_hbm, shift_hbm, packed_ref, pick_ref, affine_ref, routes_ref, logits_ref, tokens_ref, wide, sems):
     top_count, rows = routes_ref.shape
     slots = pick_ref.shape[0]
     experts = slots // capacity
@@ -76,7 +80,6 @@
             (tokens_hbm, tokens_ref),
             (gain_hbm, affine_ref.at[0:blocks]),
             (shift_hbm, affine_ref.at[blocks : 2 * blocks]),
-            (gate_hbm, gate_ref),
         ),
         sems,
     )
@@ -227,30 +230,28 @@
     bf16, f32 = jnp.bfloat16, jnp.float32
     vmem, hbm = pltpu.VMEM, pltpu.HBM
 
-    packed, pick, affine, gate_weight, routes, gate_logits = in_kernel(
+    packed, pick, affine, routes, gate_logits = in_kernel(
         "pack",
         functools.partial(pack_kernel, capacity, ring_order()[0]),
         [
             (tiles, bf16),
             ((slots, rows), bf16),
             ((2 * blocks, lanes), f32),
-            (gate_weight.shape, bf16),
             ((top_count, rows), jnp.int32),
             ((top_count, rows), f32),
         ],
         scratch=[
             pltpu.VMEM(tokens.shape, bf16),
             pltpu.VMEM(tiles, f32),
-            pltpu.SemaphoreType.DMA((6,)),
+            pltpu.SemaphoreType.DMA((5,)),
         ],
-        kinds=[hbm] * 6,
+        kinds=[hbm] * 5,
     )(
         in_hbm(routes.T),
         in_hbm(gate_logits.T),
         in_hbm(tokens),
         in_hbm(norm_gain.reshape(blocks, lanes)),
         in_hbm(norm_shift.reshape(blocks, lanes)),
-        in_hbm(gate_weight),
     )
     arrived = exchange(packed.reshape(wire)).reshape(tiles)
     arrived, affine = lax.optimization_barrier((arrived, affine))
@@ -276,7 +277,16 @@
             pltpu.SemaphoreType.DMA((2,)),
         ],
         kinds=[vmem] * 7 + [hbm],
-    )(rows_own, own_sums, other, affine, other_affine, gate_weight, up_weight, in_hbm(down_weight))
+    )(
+        rows_own,
+        own_sums,
+        other,
+        affine,
+        other_affine,
+        in_vmem(gate_weight),
+        up_weight,
+        in_hbm(down_weight),
+    )
     kept, high, low = in_kernel(
         "kept",
         functools.partial(kept_kernel, capacity, ring_order()[0]),

time: 143 us -> 142 us (level)
  no operation moved by 1% of the time
where the time goes in v7:
time: 142 us
  blocking collectives  133 us (94%)
  Pallas kernels  6 us (4%)
    all_to_all x2, blocking collectives, exchange(): lax.all_to_all(x, 'ep', split_axis=0, concat_axis=0, axis_index_groups=[r...  133 us
  transfers between devices with their start and end apart: 3, of which 1 were waited for; matrix products, arithmetic and copies ran while one was open for 0% of the time, Pallas kernels for 1%

profile of v7, /device:TPU:166, one launch (start us, length us, event | category | flops | bytes accessed | tf_op | source)
XLA Modules:
  0.0 142.0 jit_solution(15470463976997717442)
XLA Ops:
  0.0 0.0 copy-start
  0.0 1.4 %pack.1 = (bf16[1536,128]{1,0:T(8,128)(2,1)S(1)}, bf16[192,32]{1,0:T(8,128)(2,1)S(1)}, f32[16,128]{1,0:T(8,128)S(1)}, s32[4,32]{1,0:T(4,128)S(1)}, f32[4,32]{1,0:T(4,128)S(1)}) custom-call(s32[4,32]{1,0:T(4,128)} %bitcast.17, f32[4,32]{1,0:T(4,128)} %bitcast.18, bf16[32,1024]{1,0:T(8,128)(2,1)} %tokens_hbm.1, f32[8,128]{1,0:T(8,128)} %bitcast.15, ...), custom_call_target="tpu_custom_call" | custom-call | tf_op jit(solution)/shard_map/pack/pallas_call | solution.py:233
  1.4 75.0 %all_to_all.10 = bf16[32,48,128]{2,1,0:T(8,128)(2,1)S(1)} all-to-all(bf16[32,48,128]{2,1,0:T(8,128)(2,1)S(1)} %bitcast.13), channel_id=1, replica_groups={{48,50,52,54,56,58,60,62,0,2,4,6,8,10,12,14,16,18,20,22,24,26,28,30,32,..., dimensions={0} | all-to-all | bytes 786432 | tf_op jit(solution)/shard_map/all_to_all | solution.py:26
  76.4 0.0 collective-permute-start
  76.4 0.5 collective-permute-start.1
  76.9 1.6 %own.1 = (bf16[192,1024]{1,0:T(8,128)(2,1)S(1)}, f32[384,128]{1,0:T(8,128)S(1)}, bf16[1,2048,512]{2,1,0:T(8,128)(2,1)S(1)}) custom-call(bf16[1536,128]{1,0:T(8,128)(2,1)S(1)} %bitcast.12, bf16[1,2048,512]{2,1,0:T(8,128)(2,1)} %up_hbm.1), custom_call_target="tpu_custom_call" | custom-call | tf_op jit(solution)/shard_map/own/pallas_call | solution.py:260
  78.5 0.0 collective-permute-done.1.other_affine
  78.5 0.0 collective-permute-done.other_ref
  78.5 0.0 copy-done
  78.6 2.5 %expert.1 = (bf16[192,512]{1,0:T(8,128)(2,1)S(1)}, bf16[1536,128]{1,0:T(8,128)(2,1)S(1)}, bf16[512,1024]{1,0:T(8,128)(2,1)S(1)}) custom-call(bf16[192,1024]{1,0:T(8,128)(2,1)S(1)} %get-tuple-element.24.rows_own, f32[384,128]{1,0:T(8,128)S(1)} %get-tuple-element.25.own_sums, bf16[1536,128]{1,0:T(8,128)(2,1)S(1)} %collective-permute-done.other_ref, ...), custom_call_target="tpu_custom_call" | custom-call | tf_op jit(solution)/shard_map/expert/pallas_call | solution.py:268
  81.1 0.1 collective-permute-start.2
  81.2 0.5 kept.1
  81.7 1.2 collective-permute-done.2
  82.9 0.1 add_convert_fusion
  83.0 57.7 %all_to_all.11 = bf16[32,48,128]{2,1,0:T(8,128)(2,1)S(1)} all-to-all(bf16[32,48,128]{2,1,0:T(8,128)(2,1)S(1)} %bitcast.14), channel_id=1, replica_groups={{48,50,52,54,56,58,60,62,0,2,4,6,8,10,12,14,16,18,20,22,24,26,28,30,32,..., dimensions={0} | all-to-all | bytes 786432 | tf_op jit(solution)/shard_map/all_to_all | solution.py:26
  140.7 0.2 reshape.23
  140.9 0.2 fusion.1
  141.1 0.9 fusion
Async XLA Ops:
  0.0 78.5 %copy-start = (bf16[1,2048,512]{2,1,0:T(8,128)(2,1)S(1)}, bf16[1,2048,512]{2,1,0:T(8,128)(2,1)}, u32[]{:S(2)}) copy-start(bf16[1,2048,512]{2,1,0:T(8,128)(2,1)} %gate_ref.1) | copy-start | bytes 6291460
  76.4 2.1 %collective-permute-start = (bf16[1536,128]{1,0:T(8,128)(2,1)S(1)}, bf16[1536,128]{1,0:T(8,128)(2,1)S(1)}, u32[]{:S(2)}, u32[]{:S(2)}) collective-permute-start(bf16[1536,128]{1,0:T(8,128)(2,1)S(1)} %bitcast.11), channel_id=1, source_target_pairs={{0,1},{1,0},{2,3},{3,2},{4,5},{5,4},{6,7},{7,6},{8,9},{9,8},{10,11... | collective-permute-start | bytes 1179656 | tf_op jit(solution)/shard_map/ppermute | solution.py:17
  76.4 2.1 %collective-permute-start.1 = (f32[16,128]{1,0:T(8,128)S(1)}, f32[16,128]{1,0:T(8,128)S(1)}, u32[]{:S(2)}, u32[]{:S(2)}) collective-permute-start(f32[16,128]{1,0:T(8,128)S(1)} %get-tuple-element.26.own_affine), channel_id=1, source_target_pairs={{0,1},{1,0},{2,3},{3,2},{4,5},{5,4},{6,7},{7,6},{8,9},{9,8},{10,11... | collective-permute-start | bytes 24584 | tf_op jit(solution)/shard_map/ppermute | solution.py:17
  81.1 1.8 %collective-permute-start.2 = (bf16[1536,128]{1,0:T(8,128)(2,1)S(1)}, bf16[1536,128]{1,0:T(8,128)(2,1)S(1)}, u32[]{:S(2)}, u32[]{:S(2)}) collective-permute-start(bf16[1536,128]{1,0:T(8,128)(2,1)S(1)} %get-tuple-element.35), channel_id=1, source_target_pairs={{0,1},{1,0},{2,3},{3,2},{4,5},{5,4},{6,7},{7,6},{8,9},{9,8},{10,11... | collective-permute-start | bytes 1179656 | tf_op jit(solution)/shard_map/ppermute | solution.py:17

commit v8 on v7

--- a/solution.py
+++ b/solution.py
@@ -130,7 +130,9 @@
 
 
 def own_kernel(own_ref, up_hbm, rows_ref, sums_ref, up_ref, wide, sems):
-    copies = start_all(((up_hbm, up_ref),), sems)
+    width = rows_ref.shape[1]
+    here = pl.multiple_of(lax.axis_index("tp") * width, width)
+    copies = start_all(((up_hbm.at[0, pl.ds(here, width), :], up_ref),), sems)
     unpack(own_ref, rows_ref, sums_ref, wide)
     copies[0].wait()
 
@@ -143,7 +145,7 @@
     out_ref[...] = wide[...].astype(jnp.bfloat16)
 
 
-def expert_kernel(rows_own, own_sums, other_ref, own_affine, other_affine, gate_ref, up_ref, down_hbm, hidden_ref, given_ref, down_kept, wide, rows_other, other_sums, down_given, sems):
+def expert_kernel(rows_own, own_sums, other_ref, own_affine, other_affine, gate_ref, up_own, up_hbm, down_hbm, hidden_ref, given_ref, down_kept, wide, rows_other, other_sums, up_other, down_given, sems):
     slots, width = rows_own.shape
     blocks = width // lanes
     half = lax.axis_index("tp")
@@ -151,6 +153,7 @@
     there = pl.multiple_of((1 - half) * width, width)
     copies = start_all(
         (
+            (up_hbm.at[0, pl.ds(there, width), :], up_other),
             (down_hbm.at[0, :, pl.ds(there, width)], down_given),
             (down_hbm.at[0, :, pl.ds(here, width)], down_kept),
         ),
@@ -180,22 +183,22 @@
     own = normalised(rows_own, own_affine)
     other = normalised(rows_other, other_affine)
 
-    def project(weight_ref):
-        return jnp.dot(
-            own, weight_ref[0, pl.ds(here, width), :], preferred_element_type=jnp.float32
-        ) + jnp.dot(
-            other, weight_ref[0, pl.ds(there, width), :], preferred_element_type=jnp.float32
+    def project(own_weight, other_weight):
+        return jnp.dot(own, own_weight, preferred_element_type=jnp.float32) + jnp.dot(
+            other, other_weight, preferred_element_type=jnp.float32
         )
 
-    gate_cut = jnp.minimum(project(gate_ref), clamp_limit)
-    up_cut = jnp.clip(project(up_ref), -clamp_limit, clamp_limit)
+    gate_pre = project(gate_ref[0, pl.ds(here, width), :], gate_ref[0, pl.ds(there, width), :])
+    gate_cut = jnp.minimum(gate_pre, clamp_limit)
+    copies[0].wait()
+    up_cut = jnp.clip(project(up_own[...], up_other[...]), -clamp_limit, clamp_limit)
     hidden = ((up_cut + 1.0) * gate_cut * jax.nn.sigmoid(sigmoid_slope * gate_cut)).astype(
         jnp.bfloat16
     )
     hidden_ref[...] = hidden
-    copies[0].wait()
+    copies[1].wait()
     give(jnp.dot(hidden, down_given[...], preferred_element_type=jnp.float32), wide, given_ref)
-    copies[1].wait()
+    copies[2].wait()
 
 
 def kept_kernel(capacity, first_expert, hidden_ref, down_ref, routes_ref, logits_ref, pick_ref, kept_ref, high_ref, low_ref, wide):
@@ -257,10 +260,11 @@
     arrived, affine = lax.optimization_barrier((arrived, affine))
     other = swap_tp(arrived)
     other_affine = swap_tp(affine)
-    rows_own, own_sums, up_weight = in_kernel(
+    up_half = (width, up_weight.shape[2])
+    rows_own, own_sums, up_own = in_kernel(
         "own",
         own_kernel,
-        [((slots, width), bf16), ((2 * slots, lanes), f32), (up_weight.shape, bf16)],
+        [((slots, width), bf16), ((2 * slots, lanes), f32), (up_half, bf16)],
         scratch=[pltpu.VMEM(tiles, f32), pltpu.SemaphoreType.DMA((1,))],
         kinds=[vmem, hbm],
     )(arrived, in_hbm(up_weight))
@@ -273,10 +277,11 @@
             pltpu.VMEM(tiles, f32),
             pltpu.VMEM((slots, width), bf16),
             pltpu.VMEM((2 * slots, lanes), f32),
+            pltpu.VMEM(up_half, bf16),
             pltpu.VMEM(down_half, bf16),
-            pltpu.SemaphoreType.DMA((2,)),
+            pltpu.SemaphoreType.DMA((3,)),
         ],
-        kinds=[vmem] * 7 + [hbm],
+        kinds=[vmem] * 7 + [hbm] * 2,
     )(
         rows_own,
         own_sums,
@@ -284,7 +289,8 @@
         affine,
         other_affine,
         in_vmem(gate_weight),
-        up_weight,
+        up_own,
+        in_hbm(up_weight),
         in_hbm(down_weight),
     )
     kept, high, low = in_kernel(

time: 142 us -> 142 us (level)
  no operation moved by 1% of the time
where the time goes in v8:
time: 142 us
  blocking collectives  133 us (94%)
  Pallas kernels  6.09 us (4%)
    all_to_all x2, blocking collectives, exchange(): lax.all_to_all(x, 'ep', split_axis=0, concat_axis=0, axis_index_groups=[r...  133 us
    pallas_call x1, Pallas kernels, body(): in_kernel('expert', expert_kernel, [((slots, gate_weight.shape[2]), bf16)...  2.97 us
  transfers between devices with their start and end apart: 3, of which 1 were waited for; matrix products, arithmetic and copies ran while one was open for 0% of the time, Pallas kernels for 1%

profile of v8, /device:TPU:166, one launch (start us, length us, event | category | flops | bytes accessed | tf_op | source)
XLA Modules:
  0.0 142.1 jit_solution(12665308749779538872)
XLA Ops:
  0.0 0.0 copy-start
  0.0 1.4 %pack.1 = (bf16[1536,128]{1,0:T(8,128)(2,1)S(1)}, bf16[192,32]{1,0:T(8,128)(2,1)S(1)}, f32[16,128]{1,0:T(8,128)S(1)}, s32[4,32]{1,0:T(4,128)S(1)}, f32[4,32]{1,0:T(4,128)S(1)}) custom-call(s32[4,32]{1,0:T(4,128)} %bitcast.17, f32[4,32]{1,0:T(4,128)} %bitcast.18, bf16[32,1024]{1,0:T(8,128)(2,1)} %tokens_hbm.1, f32[8,128]{1,0:T(8,128)} %bitcast.15, ...), custom_call_target="tpu_custom_call" | custom-call | tf_op jit(solution)/shard_map/pack/pallas_call | solution.py:236
  1.4 75.0 %all_to_all.10 = bf16[32,48,128]{2,1,0:T(8,128)(2,1)S(1)} all-to-all(bf16[32,48,128]{2,1,0:T(8,128)(2,1)S(1)} %bitcast.13), channel_id=1, replica_groups={{48,50,52,54,56,58,60,62,0,2,4,6,8,10,12,14,16,18,20,22,24,26,28,30,32,..., dimensions={0} | all-to-all | bytes 786432 | tf_op jit(solution)/shard_map/all_to_all | solution.py:26
  76.4 0.0 collective-permute-start
  76.4 0.5 collective-permute-start.1
  76.9 1.2 own.1
  78.2 0.0 collective-permute-done.1.other_affine
  78.2 0.0 collective-permute-done.other_ref
  78.2 0.0 copy-done
  78.2 3.0 %expert.1 = (bf16[192,512]{1,0:T(8,128)(2,1)S(1)}, bf16[1536,128]{1,0:T(8,128)(2,1)S(1)}, bf16[512,1024]{1,0:T(8,128)(2,1)S(1)}) custom-call(bf16[192,1024]{1,0:T(8,128)(2,1)S(1)} %get-tuple-element.24.rows_own, f32[384,128]{1,0:T(8,128)S(1)} %get-tuple-element.25.own_sums, bf16[1536,128]{1,0:T(8,128)(2,1)S(1)} %collective-permute-done.other_ref, ...), custom_call_target="tpu_custom_call" | custom-call | tf_op jit(solution)/shard_map/expert/pallas_call | solution.py:272
  81.2 0.2 collective-permute-start.2
  81.4 0.4 kept.1
  81.8 1.2 collective-permute-done.2
  83.0 0.1 add_convert_fusion
  83.1 57.7 %all_to_all.11 = bf16[32,48,128]{2,1,0:T(8,128)(2,1)S(1)} all-to-all(bf16[32,48,128]{2,1,0:T(8,128)(2,1)S(1)} %bitcast.14), channel_id=1, replica_groups={{48,50,52,54,56,58,60,62,0,2,4,6,8,10,12,14,16,18,20,22,24,26,28,30,32,..., dimensions={0} | all-to-all | bytes 786432 | tf_op jit(solution)/shard_map/all_to_all | solution.py:26
  140.8 0.2 reshape.23
  141.0 0.2 fusion.1
  141.2 0.9 fusion
Async XLA Ops:
  0.0 78.2 %copy-start = (bf16[1,2048,512]{2,1,0:T(8,128)(2,1)S(1)}, bf16[1,2048,512]{2,1,0:T(8,128)(2,1)}, u32[]{:S(2)}) copy-start(bf16[1,2048,512]{2,1,0:T(8,128)(2,1)} %gate_ref.1) | copy-start | bytes 6291460
  76.4 1.8 %collective-permute-start = (bf16[1536,128]{1,0:T(8,128)(2,1)S(1)}, bf16[1536,128]{1,0:T(8,128)(2,1)S(1)}, u32[]{:S(2)}, u32[]{:S(2)}) collective-permute-start(bf16[1536,128]{1,0:T(8,128)(2,1)S(1)} %bitcast.11), channel_id=1, source_target_pairs={{0,1},{1,0},{2,3},{3,2},{4,5},{5,4},{6,7},{7,6},{8,9},{9,8},{10,11... | collective-permute-start | bytes 1179656 | tf_op jit(solution)/shard_map/ppermute | solution.py:17
  76.4 1.8 %collective-permute-start.1 = (f32[16,128]{1,0:T(8,128)S(1)}, f32[16,128]{1,0:T(8,128)S(1)}, u32[]{:S(2)}, u32[]{:S(2)}) collective-permute-start(f32[16,128]{1,0:T(8,128)S(1)} %get-tuple-element.26.own_affine), channel_id=1, source_target_pairs={{0,1},{1,0},{2,3},{3,2},{4,5},{5,4},{6,7},{7,6},{8,9},{9,8},{10,11... | collective-permute-start | bytes 24584 | tf_op jit(solution)/shard_map/ppermute | solution.py:17
  81.2 1.8 %collective-permute-start.2 = (bf16[1536,128]{1,0:T(8,128)(2,1)S(1)}, bf16[1536,128]{1,0:T(8,128)(2,1)S(1)}, u32[]{:S(2)}, u32[]{:S(2)}) collective-permute-start(bf16[1536,128]{1,0:T(8,128)(2,1)S(1)} %get-tuple-element.35), channel_id=1, source_target_pairs={{0,1},{1,0},{2,3},{3,2},{4,5},{5,4},{6,7},{7,6},{8,9},{9,8},{10,11... | collective-permute-start | bytes 1179656 | tf_op jit(solution)/shard_map/ppermute | solution.py:17

commit v9 on v7

--- a/solution.py
+++ b/solution.py
@@ -19,7 +19,7 @@
 
 def ring_order():
     count = lax.axis_size("ep")
-    return [(3 * count // 4 + k) % count for k in range(count)]
+    return [(5 * count // 8 + k) % count for k in range(count)]
 
 
 def exchange(x):

time: 142 us -> 142 us (level)
  no operation moved by 1% of the time
where the time goes in v9:
time: 142 us; the launch traced here: 141 us
  blocking collectives  132 us (93%)
  Pallas kernels  6 us (4%)
    all_to_all x2, blocking collectives, exchange(): lax.all_to_all(x, 'ep', split_axis=0, concat_axis=0, axis_index_groups=[r...  132 us
  transfers between devices with their start and end apart: 3, of which 1 were waited for; matrix products, arithmetic and copies ran while one was open for 0% of the time, Pallas kernels for 1%

profile of v9, /device:TPU:166, one launch (start us, length us, event | category | flops | bytes accessed | tf_op | source)
XLA Modules:
  0.0 141.0 jit_solution(6213769474661764216)
XLA Ops:
  0.0 0.0 copy-start
  0.0 1.4 %pack.1 = (bf16[1536,128]{1,0:T(8,128)(2,1)S(1)}, bf16[192,32]{1,0:T(8,128)(2,1)S(1)}, f32[16,128]{1,0:T(8,128)S(1)}, s32[4,32]{1,0:T(4,128)S(1)}, f32[4,32]{1,0:T(4,128)S(1)}) custom-call(s32[4,32]{1,0:T(4,128)} %bitcast.17, f32[4,32]{1,0:T(4,128)} %bitcast.18, bf16[32,1024]{1,0:T(8,128)(2,1)} %tokens_hbm.1, f32[8,128]{1,0:T(8,128)} %bitcast.15, ...), custom_call_target="tpu_custom_call" | custom-call | tf_op jit(solution)/shard_map/pack/pallas_call | solution.py:233
  1.4 74.1 %all_to_all.10 = bf16[32,48,128]{2,1,0:T(8,128)(2,1)S(1)} all-to-all(bf16[32,48,128]{2,1,0:T(8,128)(2,1)S(1)} %bitcast.13), channel_id=1, replica_groups={{40,42,44,46,48,50,52,54,56,58,60,62,0,2,4,6,8,10,12,14,16,18,20,22,24,..., dimensions={0} | all-to-all | bytes 786432 | tf_op jit(solution)/shard_map/all_to_all | solution.py:26
  75.5 0.0 collective-permute-start
  75.5 0.5 collective-permute-start.1
  76.0 1.6 %own.1 = (bf16[192,1024]{1,0:T(8,128)(2,1)S(1)}, f32[384,128]{1,0:T(8,128)S(1)}, bf16[1,2048,512]{2,1,0:T(8,128)(2,1)S(1)}) custom-call(bf16[1536,128]{1,0:T(8,128)(2,1)S(1)} %bitcast.12, bf16[1,2048,512]{2,1,0:T(8,128)(2,1)} %up_hbm.1), custom_call_target="tpu_custom_call" | custom-call | tf_op jit(solution)/shard_map/own/pallas_call | solution.py:260
  77.7 0.0 collective-permute-done.1.other_affine
  77.7 0.0 collective-permute-done.other_ref
  77.7 0.0 copy-done
  77.7 2.5 %expert.1 = (bf16[192,512]{1,0:T(8,128)(2,1)S(1)}, bf16[1536,128]{1,0:T(8,128)(2,1)S(1)}, bf16[512,1024]{1,0:T(8,128)(2,1)S(1)}) custom-call(bf16[192,1024]{1,0:T(8,128)(2,1)S(1)} %get-tuple-element.24.rows_own, f32[384,128]{1,0:T(8,128)S(1)} %get-tuple-element.25.own_sums, bf16[1536,128]{1,0:T(8,128)(2,1)S(1)} %collective-permute-done.other_ref, ...), custom_call_target="tpu_custom_call" | custom-call | tf_op jit(solution)/shard_map/expert/pallas_call | solution.py:268
  80.2 0.1 collective-permute-start.2
  80.4 0.5 kept.1
  80.8 1.2 collective-permute-done.2
  82.1 0.1 add_convert_fusion
  82.2 57.6 %all_to_all.11 = bf16[32,48,128]{2,1,0:T(8,128)(2,1)S(1)} all-to-all(bf16[32,48,128]{2,1,0:T(8,128)(2,1)S(1)} %bitcast.14), channel_id=1, replica_groups={{40,42,44,46,48,50,52,54,56,58,60,62,0,2,4,6,8,10,12,14,16,18,20,22,24,..., dimensions={0} | all-to-all | bytes 786432 | tf_op jit(solution)/shard_map/all_to_all | solution.py:26
  139.8 0.2 reshape.23
  139.9 0.2 fusion.1
  140.1 0.9 fusion
Async XLA Ops:
  0.0 77.7 %copy-start = (bf16[1,2048,512]{2,1,0:T(8,128)(2,1)S(1)}, bf16[1,2048,512]{2,1,0:T(8,128)(2,1)}, u32[]{:S(2)}) copy-start(bf16[1,2048,512]{2,1,0:T(8,128)(2,1)} %gate_ref.1) | copy-start | bytes 6291460
  75.5 2.1 %collective-permute-start = (bf16[1536,128]{1,0:T(8,128)(2,1)S(1)}, bf16[1536,128]{1,0:T(8,128)(2,1)S(1)}, u32[]{:S(2)}, u32[]{:S(2)}) collective-permute-start(bf16[1536,128]{1,0:T(8,128)(2,1)S(1)} %bitcast.11), channel_id=1, source_target_pairs={{0,1},{1,0},{2,3},{3,2},{4,5},{5,4},{6,7},{7,6},{8,9},{9,8},{10,11... | collective-permute-start | bytes 1179656 | tf_op jit(solution)/shard_map/ppermute | solution.py:17
  75.5 2.1 %collective-permute-start.1 = (f32[16,128]{1,0:T(8,128)S(1)}, f32[16,128]{1,0:T(8,128)S(1)}, u32[]{:S(2)}, u32[]{:S(2)}) collective-permute-start(f32[16,128]{1,0:T(8,128)S(1)} %get-tuple-element.26.own_affine), channel_id=1, source_target_pairs={{0,1},{1,0},{2,3},{3,2},{4,5},{5,4},{6,7},{7,6},{8,9},{9,8},{10,11... | collective-permute-start | bytes 24584 | tf_op jit(solution)/shard_map/ppermute | solution.py:17
  80.2 1.8 %collective-permute-start.2 = (bf16[1536,128]{1,0:T(8,128)(2,1)S(1)}, bf16[1536,128]{1,0:T(8,128)(2,1)S(1)}, u32[]{:S(2)}, u32[]{:S(2)}) collective-permute-start(bf16[1536,128]{1,0:T(8,128)(2,1)S(1)} %get-tuple-element.35), channel_id=1, source_target_pairs={{0,1},{1,0},{2,3},{3,2},{4,5},{5,4},{6,7},{7,6},{8,9},{9,8},{10,11... | collective-permute-start | bytes 1179656 | tf_op jit(solution)/shard_map/ppermute | solution.py:17
